TPU v7x, 32 devices: a whole 2x2x4 slice. The times are simulated.
32 devices in a mesh: sp: 8 (over z, x), tp: 4 (over y, core).
Axes of the slice: x: 2, y: 2, z: 4, core: 2. Of those that a mesh axis runs over, the one named last changes fastest.
Arguments:
- tokens: bfloat16 [2048, 3072], P('sp', 'tp'), may hold values from -6 to 6
- norm_gain: float32 [3072], replicated, may hold values from 0.1 to 1.9
- state_in_weight: bfloat16 [3072, 1024], P('sp', 'tp'), may hold values from -0.109375 to 0.109375
- pool_in_weight: bfloat16 [3072, 1024], P('sp', 'tp'), may hold values from -0.109375 to 0.109375
- rate_real: float32 [64, 64], replicated, may hold values from -1.5 to -0.5
- rate_imag: float32 [64, 64], replicated, may hold values from 0 to 200
- log_step: float32 [64], replicated, may hold values from -2 to 0.7
- input_real: float32 [64, 64, 16], replicated, may hold values from -1 to 1
- input_imag: float32 [64, 64, 16], replicated, may hold values from -1 to 1
- output_real: float32 [64, 16, 64], replicated, may hold values from -64 to 64
- output_imag: float32 [64, 16, 64], replicated, may hold values from -64 to 64
- skip_gain: float32 [1024], replicated, may hold values from -3 to 3
- pool_weight: bfloat16 [16, 64, 64], replicated, may hold values from -0.75 to 0.75
- pool_gain: float32 [1024], replicated, may hold values from 0.1 to 1.9
- state_out_weight: bfloat16 [1024, 3072], P('sp', 'tp'), may hold values from -0.125 to 0.125
- pool_out_weight: bfloat16 [1024, 3072], P('sp', 'tp'), may hold values from -0.125 to 0.125
Outputs:
- mixer_output: bfloat16 [2048, 3072], P('sp', 'tp')
All inputs are finite; a program needn't handle non-finite values.
Results may differ from a plain program's by a relative error of at most 0.0065.
Values may be sent and summed in bfloat16 or wider, within the bound.
A program may use at most 64 MiB of HBM per device.

v0:
```python
import functools

import jax
import jax.numpy as jnp
from jax import lax
from jax.experimental import pallas as pl
from jax.experimental.pallas import tpu as pltpu
from jax.sharding import PartitionSpec as P

SSM_GROUP = 16
POOL_GROUP = 64
CHUNKS = 8
PIECES = 2

epsilon = 1e-06
window_reach = 16
f32, bf16 = jnp.float32, jnp.bfloat16
MESH = pl.DeviceIdType.MESH


def discretize(rate_real, rate_imag, log_step, length):
    step_size = jnp.exp(log_step)[:, None] / length
    exponent = rate_real * step_size
    angle = rate_imag * step_size
    magnitude = jnp.exp(exponent)
    decay_real = magnitude * jnp.cos(angle)
    decay_imag = magnitude * jnp.sin(angle)
    less_one = jnp.expm1(exponent) * jnp.cos(angle) - 2.0 * jnp.square(jnp.sin(0.5 * angle))
    denominator = rate_real * rate_real + rate_imag * rate_imag
    factor_real = (less_one * rate_real + decay_imag * rate_imag) / denominator
    factor_imag = (decay_imag * rate_real - less_one * rate_imag) / denominator
    return decay_real, decay_imag, factor_real, factor_imag


def iota(shape, axis):
    return lax.broadcasted_iota(jnp.int32, shape, axis)


def dot(a, b):
    return jnp.dot(a, b, preferred_element_type=f32)


def dot_nt(a, b):
    return lax.dot_general(a, b, (((1,), (1,)), ((), ())), preferred_element_type=f32)


def split(a):
    high = a.astype(bf16)
    return high, (a - high.astype(f32)).astype(bf16)


def cmul(ar, ai, br, bi):
    return ar * br - ai * bi, ar * bi + ai * br


def kernel(
    n_sp, n_tp, n_x, states,
    tok_ref, gain_ref, wsi_ref, wpi_ref, rr_ref, ri_ref, step_ref, inr_ref, ini_ref, outr_ref,
    outi_ref, skip_ref, pw_ref, pg_ref, wso_ref, wpo_ref,
    out_ref,
    tok_full, wsi, wpi, wso, wpo, scaled, dmat, rmat, pmat, push, ext, halo, ends, act,
    mine_s, mine_p, halo_out, rates, matrices, pool_own, dec_ref,
    own_sem, ring_send, ring_recv, tok_send, tok_recv, act_send, act_recv, halo_sem, end_send, end_recv,
):
    me, tp = lax.axis_index("sp"), lax.axis_index("tp")
    n_z = n_sp // n_x
    rows = tok_ref.shape[0]
    features = tok_ref.shape[1]
    width = wsi_ref.shape[1]
    pool_width = wpi_ref.shape[1]
    groups = width // SSM_GROUP
    columns = groups * states
    pool_groups = pool_width // POOL_GROUP
    span = rows // CHUNKS

    def place(p):
        x, r = p // n_z, p % n_z
        return (r + (x % 2) * (n_z - 1 - 2 * r)) * n_x + x

    my_x, my_z = me % n_x, me // n_x
    at = my_x * n_z + my_z + (my_x % 2) * (n_z - 1 - 2 * my_z)

    barrier = pltpu.get_barrier_semaphore()
    for k in range(1, n_sp):
        pl.semaphore_signal(barrier, inc=1, device_id=((me + k) % n_sp, tp), device_id_type=MESH)
    for k in range(1, n_tp):
        pl.semaphore_signal(barrier, inc=1, device_id=(me, (tp + k) % n_tp), device_id_type=MESH)

    fulls = ((wsi_ref, wsi), (wpi_ref, wpi), (wso_ref, wso), (wpo_ref, wpo))
    owns = []
    for a, (own, full) in enumerate(fulls):
        count = own.shape[0]
        owns.append(
            pltpu.make_async_copy(
                own, full.at[pl.ds(pl.multiple_of(me * count, count), count)], own_sem.at[a]
            )
        )
    owns.append(pltpu.make_async_copy(tok_ref, tok_full.at[tp], own_sem.at[4]))
    def heads(ref, count):
        return ref.at[pl.ds(pl.multiple_of(tp * count, count), count)]

    loads = [
        pltpu.make_async_copy(heads(ref, groups), there, own_sem.at[5 + k])
        for k, (ref, there) in enumerate(
            (
                (rr_ref, rates.at[0]), (ri_ref, rates.at[1]), (inr_ref, matrices.at[0]),
                (ini_ref, matrices.at[1]), (outr_ref, matrices.at[2]), (outi_ref, matrices.at[3]),
            )
        )
    ]
    loads.append(pltpu.make_async_copy(heads(pw_ref, pool_groups), pool_own, own_sem.at[11]))
    for c in owns + loads:
        c.start()
    pl.semaphore_wait(barrier, n_sp - 1 + n_tp - 1)

    ways = (1, -1)

    def reach_of(a, d):
        return n_sp // 2 if a % 2 == d else n_sp - 1 - n_sp // 2

    def part(a, d, s, h):
        own, full = fulls[a]
        count = own.shape[0]
        size = count // PIECES
        way = ways[d]
        owner = place((at - way * s + n_sp) % n_sp)
        there = full.at[pl.ds(pl.multiple_of(owner * count + h * size, size), size)]
        source = own.at[pl.ds(h * size, size)] if s == 0 else there
        return source, there, (place((at + way + n_sp) % n_sp), tp)

    def sender(a, d, s, h):
        source, there, target = part(a, d, s, h)
        return pltpu.make_async_remote_copy(
            source, there, ring_send.at[a, d, s, h], ring_recv.at[a, d, s, h],
            device_id=target, device_id_type=MESH,
        )

    def arrive(a, d, s, h):
        _, there, target = part(a, d, s + 1, h)
        pltpu.make_async_remote_copy(
            there, there, ring_send.at[a, d, s, h], ring_recv.at[a, d, s, h],
            device_id=target, device_id_type=MESH,
        ).wait_recv()

    longest = n_sp // 2

    def ring(phase, s, h):
        streams = [
            (a, d) for a in (2 * phase, 2 * phase + 1) for d in range(2) if s < reach_of(a, d)
        ]
        for a, d in sorted(streams, key=lambda i: -reach_of(*i)):
            arrive(a, d, s, h)
            if s + 1 < reach_of(a, d):
                sender(a, d, s + 1, h).start()
        if phase == 0 and h == PIECES - 1:
            for a, d in streams:
                if s + 1 == reach_of(a, d):
                    for g in range(PIECES):
                        sender(a + 2, d, 0, g).start()

    turns = [(phase, s, h) for phase in range(2) for s in range(longest) for h in range(PIECES)]
    turn = [0]

    def step(stop=len(turns)):
        if turn[0] < stop:
            ring(*turns[turn[0]])
            turn[0] += 1

    def token_copy(k):
        return pltpu.make_async_remote_copy(
            tok_ref, tok_full.at[tp], tok_send.at[k - 1], tok_recv.at[k - 1],
            device_id=(me, (tp + k) % n_tp), device_id_type=MESH,
        )

    for h in range(PIECES):
        for a, d in ((0, 0), (1, 1), (0, 1), (1, 0)):
            sender(a, d, 0, h).start()
    for k in range(1, n_tp):
        token_copy(k).start()

    tile = iota((states, columns), 0) == iota((states, columns), 1) % states
    tile_exact, tile_half = tile.astype(f32), tile.astype(bf16)

    def exactly(a, b):
        return jnp.dot(a, b, precision=lax.Precision.HIGHEST, preferred_element_type=f32)

    factors = []

    def build_decay():
        for c in loads:
            c.wait()
        own_head = iota((groups, columns), 0) == iota((groups, columns), 1) // states

        def flat(a):
            return jnp.sum(jnp.where(own_head, exactly(a, tile_exact), 0.0), axis=0, keepdims=True)

        rate_real, rate_imag = flat(rates[0]), flat(rates[1])
        all_groups = step_ref.shape[1]
        head = iota((all_groups, columns), 0) == tp * groups + iota((all_groups, columns), 1) // states
        log_step = exactly(jnp.broadcast_to(step_ref[...], (8, all_groups)), head.astype(f32))[0:1]
        step_size = jnp.exp(log_step) / (rows * n_sp)
        exponent, angle = rate_real * step_size, rate_imag * step_size
        magnitude = jnp.exp(exponent)
        cosine = jnp.cos(angle)
        decay_real, decay_imag = magnitude * cosine, magnitude * jnp.sin(angle)
        series = jnp.ones_like(exponent)
        for k in range(10, 1, -1):
            series = 1.0 + series * exponent * (1.0 / k)
        growth = jnp.where(jnp.abs(exponent) < 0.5, exponent * series, magnitude - 1.0)
        less_one = growth * cosine - 2.0 * jnp.square(jnp.sin(0.5 * angle))
        denominator = rate_real * rate_real + rate_imag * rate_imag
        factors.append((less_one * rate_real + decay_imag * rate_imag) / denominator)
        factors.append((decay_imag * rate_real - less_one * rate_imag) / denominator)
        dec_ref[0:1, :] = decay_real
        dec_ref[1:2, :] = decay_imag

    def spread(k):
        high, low = split(matrices[k].reshape(width, states))
        return dot(high, tile_half) + dot(low, tile_half)

    def build_drive(i):
        same = iota((width, columns), 0) // SSM_GROUP == iota((width, columns), 1) // states
        real, imag = spread(0), spread(1)
        if i == 0:
            drive = factors[0] * real - factors[1] * imag
        else:
            drive = factors[0] * imag + factors[1] * real
        for j, piece in enumerate(split(jnp.where(same, drive, 0.0))):
            dmat[i, j] = piece

    def build_read(i):
        across = (iota((columns, states), 0) % states == iota((columns, states), 1)).astype(bf16)
        same = iota((columns, width), 0) // states == iota((columns, width), 1) // SSM_GROUP
        for j, piece in enumerate(split(matrices[2 + i].reshape(width, states))):
            rmat[i, j] = jnp.where(same, dot_nt(across, piece), 0.0).astype(bf16)

    def build_pool():
        across = (
            iota((POOL_GROUP, pool_width), 0) == iota((POOL_GROUP, pool_width), 1) % POOL_GROUP
        ).astype(bf16)
        same = iota((pool_width, pool_width), 0) // POOL_GROUP == iota((pool_width, pool_width), 1) // POOL_GROUP
        own = pool_own[...].reshape(pool_width, POOL_GROUP)
        pmat[...] = jnp.where(same, dot(own, across), 0.0).astype(bf16)

    squares = []

    def take(t):
        block = tok_full[t].astype(f32)
        squares.append(jnp.sum(block * block, axis=1, keepdims=True))
        cut = slice(t * features, (t + 1) * features)
        scaled[:, cut] = (block * gain_ref[:, cut]).astype(bf16)

    def tokens_in():
        owns[4].wait()
        for k in range(1, n_tp):
            pltpu.make_async_remote_copy(
                tok_ref, tok_full.at[(tp - k + n_tp) % n_tp], tok_send.at[k - 1], tok_recv.at[k - 1],
                device_id=(me, (tp + k) % n_tp), device_id_type=MESH,
            ).wait_recv()

    half = len(turns) // 2
    for at_work, work in enumerate(
        (
            build_decay, lambda: build_drive(0), lambda: build_drive(1), lambda: build_read(0),
            lambda: build_read(1), build_pool,
        )
    ):
        work()
        if at_work in (0, 1, 3, 5):
            step(half)
    while turn[0] < half - 3:
        step(half)
    tokens_in()
    for t in range(n_tp):
        take(t)
        if t == n_tp // 2 - 1:
            step(half)
    while turn[0] < half:
        step(half)
    owns[0].wait()
    owns[1].wait()
    inverse = lax.rsqrt(sum(squares) / (features * n_tp) + epsilon)
    state_in = (dot(scaled[...], wsi[...]) * inverse).astype(bf16)
    pool_in = (dot(scaled[...], wpi[...]) * inverse).astype(bf16)
    ext[window_reach:] = pool_in
    halo_out[...] = pool_in[rows - window_reach :]
    halo_copy = pltpu.make_async_remote_copy(
        halo_out, halo, halo_sem.at[0], halo_sem.at[1],
        device_id=((me + 1) % n_sp, tp), device_id_type=MESH,
    )
    shuffle = (
        iota((rows, rows), 1)
        == (iota((rows, rows), 0) % CHUNKS) * span + iota((rows, rows), 0) // CHUNKS
    ).astype(bf16)
    signal = dot(shuffle, state_in).astype(bf16)
    for i in range(2):
        push[i] = dot(signal, dmat[i, 0]) + dot(signal, dmat[i, 1])
        if i == 0:
            halo_copy.start()
        else:
            step()
    decay_real = jnp.broadcast_to(dec_ref[0:1, :], (CHUNKS, columns))
    decay_imag = jnp.broadcast_to(dec_ref[1:2, :], (CHUNKS, columns))

    def advance(p, carry):
        cut = pl.ds(pl.multiple_of(p * CHUNKS, CHUNKS), CHUNKS)
        real, imag = cmul(decay_real, decay_imag, *carry)
        real, imag = real + push[0, cut, :], imag + push[1, cut, :]
        push[0, cut, :] = real
        push[1, cut, :] = imag
        return real, imag

    zero = jnp.zeros((CHUNKS, columns), f32)
    end_real, end_imag = lax.fori_loop(0, span, advance, (zero, zero))

    def power(real, imag, count):
        out = None
        while count:
            if count % 2:
                out = (real, imag) if out is None else cmul(*out, real, imag)
            real, imag = cmul(real, imag, real, imag)
            count //= 2
        return out

    chunk_decay = power(dec_ref[0:1, :], dec_ref[1:2, :], span)
    block_decay = power(*chunk_decay, CHUNKS)
    row_zero = jnp.zeros((1, columns), f32)
    total = (row_zero, row_zero)
    for j in range(CHUNKS):
        moved = cmul(*chunk_decay, *total)
        total = (moved[0] + end_real[j : j + 1], moved[1] + end_imag[j : j + 1])
    which = iota((CHUNKS, columns), 0)
    ends[me] = jnp.where(which == 0, total[0], jnp.where(which == 1, total[1], 0.0))

    def end_copy(k):
        return pltpu.make_async_remote_copy(
            ends.at[me], ends.at[me], end_send.at[k - 1], end_recv.at[k - 1],
            device_id=((me + k) % n_sp, tp), device_id_type=MESH,
        )

    for k in range(1, n_sp):
        end_copy(k).start()

    halo_copy.wait_recv()
    ext[:window_reach] = jnp.where(me == 0, jnp.zeros_like(halo), halo[...])
    group = tp * (pool_width // POOL_GROUP) + iota((rows, pool_width), 1) // POOL_GROUP
    window = jnp.left_shift(jnp.ones_like(group), group % 4 + 1)
    targets = iota((rows, rows + window_reach), 0) + window_reach
    sources = iota((rows, rows + window_reach), 1)
    whole = ext[...]
    sums = jnp.zeros((rows, pool_width), f32)
    for power_index in range(1, 5):
        reach = 2**power_index
        band = ((sources <= targets) & (sources > targets - reach)).astype(bf16)
        sums = jnp.where(window == reach, dot(band, whole), sums)
        if power_index == 2:
            step()
    position = me * rows + iota((rows, pool_width), 0)
    divisor = jnp.minimum(position + 1, window).astype(f32)
    pooled = sums / divisor - ext[window_reach:].astype(f32)
    pooled_high, pooled_low = split(pooled)
    pool_gain = pg_ref[:, pl.ds(pl.multiple_of(tp * pool_width, pool_width), pool_width)]
    projected = dot(pooled_high, pmat[...]) + dot(pooled_low, pmat[...])
    mine_p[...] = (projected * pool_gain).astype(bf16)
    step()

    def act_copy(which, k, source):
        mine = mine_s if which == 0 else mine_p
        return pltpu.make_async_remote_copy(
            mine, act.at[which, source], act_send.at[which, k - 1], act_recv.at[which, k - 1],
            device_id=(me, (tp + k) % n_tp), device_id_type=MESH,
        )

    for k in range(1, n_tp):
        act_copy(1, k, tp).start()
    act[1, tp] = mine_p[...]

    for k in range(1, n_sp):
        there = ends.at[(me - k + n_sp) % n_sp]
        pltpu.make_async_remote_copy(
            there, there, end_send.at[k - 1], end_recv.at[k - 1],
            device_id=((me + k) % n_sp, tp), device_id_type=MESH,
        ).wait_recv()
    total = (row_zero, row_zero)
    for s in range(n_sp - 1):
        moved = cmul(*block_decay, *total)
        use = s < me
        total = (
            jnp.where(use, moved[0] + ends[s, 0:1, :], total[0]),
            jnp.where(use, moved[1] + ends[s, 1:2, :], total[1]),
        )
    begin_real, begin_imag = zero, zero
    for j in range(CHUNKS):
        begin_real = jnp.where(which == j, total[0], begin_real)
        begin_imag = jnp.where(which == j, total[1], begin_imag)
        moved = cmul(*chunk_decay, *total)
        total = (moved[0] + end_real[j : j + 1], moved[1] + end_imag[j : j + 1])

    def add_carry(p, carry):
        cut = pl.ds(pl.multiple_of(p * CHUNKS, CHUNKS), CHUNKS)
        real, imag = cmul(decay_real, decay_imag, *carry)
        push[0, cut, :] = push[0, cut, :] + real
        push[1, cut, :] = push[1, cut, :] + imag
        return real, imag

    lax.fori_loop(0, span, add_carry, (begin_real, begin_imag))
    step()
    real_high, real_low = split(push[0])
    imag_high, imag_low = split(push[1])
    readout = dot(real_high, rmat[0, 0]) + dot(real_high, rmat[0, 1]) + dot(real_low, rmat[0, 0])
    step()
    readout -= dot(imag_high, rmat[1, 0]) + dot(imag_high, rmat[1, 1]) + dot(imag_low, rmat[1, 0])
    skip = skip_ref[:, pl.ds(pl.multiple_of(tp * width, width), width)]
    readout += skip * signal.astype(f32)
    shuffled = jax.nn.gelu(readout).astype(bf16)
    restore = (
        iota((rows, rows), 0)
        == (iota((rows, rows), 1) % CHUNKS) * span + iota((rows, rows), 1) // CHUNKS
    ).astype(bf16)
    mine_s[...] = dot(restore, shuffled).astype(bf16)
    for k in range(1, n_tp):
        act_copy(0, k, tp).start()
    act[0, tp] = mine_s[...]
    while turn[0] < len(turns):
        step()
    for which in (1, 0):
        for k in range(1, n_tp):
            act_copy(which, k, (tp - k + n_tp) % n_tp).wait_recv()
    owns[2].wait()
    owns[3].wait()
    result = None
    for t in range(n_tp):
        for which, full, size in ((1, wpo, pool_width), (0, wso, width)):
            term = dot(act[which, t], full[t * size : (t + 1) * size, :])
            result = term if result is None else result + term
    out_ref[...] = result.astype(bf16)

    for a in range(4):
        for d in range(2):
            for s in range(reach_of(a, d)):
                for h in range(PIECES):
                    sender(a, d, s, h).wait_send()
    for k in range(1, n_tp):
        token_copy(k).wait_send()
        act_copy(0, k, tp).wait_send()
        act_copy(1, k, tp).wait_send()
    halo_copy.wait_send()
    for k in range(1, n_sp):
        end_copy(k).wait_send()


def body(
    n_sp, n_tp, n_x,
    tokens, norm_gain, state_in_weight, pool_in_weight, rate_real, rate_imag, log_step,
    input_real, input_imag, output_real, output_imag, skip_gain, pool_weight, pool_gain,
    state_out_weight, pool_out_weight,
):
    rows, features = tokens.shape
    in_rows, width = state_in_weight.shape
    pool_width = pool_in_weight.shape[1]
    out_rows, out_columns = state_out_weight.shape
    groups = width // SSM_GROUP
    states = rate_real.shape[1]
    columns = groups * states
    pool_groups = pool_width // POOL_GROUP
    vmem = pl.BlockSpec(memory_space=pltpu.VMEM)
    anywhere = pl.BlockSpec(memory_space=pl.ANY)
    dma = pltpu.SemaphoreType.DMA
    return pl.pallas_call(
        functools.partial(kernel, n_sp, n_tp, n_x, states),
        out_shape=jax.ShapeDtypeStruct((rows, out_columns), bf16),
        in_specs=[anywhere, vmem] + [anywhere] * 4 + [vmem] + [anywhere] * 4 + [vmem, anywhere, vmem]
        + [anywhere] * 2,
        out_specs=vmem,
        scratch_shapes=[
            pltpu.VMEM((n_tp, rows, features), bf16),
            pltpu.VMEM((n_sp * in_rows, width), bf16),
            pltpu.VMEM((n_sp * in_rows, pool_width), bf16),
            pltpu.VMEM((n_sp * out_rows, out_columns), bf16),
            pltpu.VMEM((n_sp * out_rows, out_columns), bf16),
            pltpu.VMEM((rows, features * n_tp), bf16),
            pltpu.VMEM((2, 2, width, columns), bf16),
            pltpu.VMEM((2, 2, columns, width), bf16),
            pltpu.VMEM((pool_width, pool_width), bf16),
            pltpu.VMEM((2, rows, columns), f32),
            pltpu.VMEM((rows + window_reach, pool_width), bf16),
            pltpu.VMEM((window_reach, pool_width), bf16),
            pltpu.VMEM((n_sp, CHUNKS, columns), f32),
            pltpu.VMEM((2, n_tp, rows, width), bf16),
            pltpu.VMEM((rows, width), bf16),
            pltpu.VMEM((rows, pool_width), bf16),
            pltpu.VMEM((window_reach, pool_width), bf16),
            pltpu.VMEM((2, groups, states), f32),
            pltpu.VMEM((4, groups, SSM_GROUP, states), f32),
            pltpu.VMEM((pool_groups, POOL_GROUP, POOL_GROUP), bf16),
            pltpu.VMEM((2, columns), f32),
            dma((12,)),
            dma((4, 2, n_sp // 2, PIECES)),
            dma((4, 2, n_sp // 2, PIECES)),
            dma((n_tp - 1,)),
            dma((n_tp - 1,)),
            dma((2, n_tp - 1)),
            dma((2, n_tp - 1)),
            dma((2,)),
            dma((n_sp - 1,)),
            dma((n_sp - 1,)),
        ],
        compiler_params=pltpu.CompilerParams(
            collective_id=0, has_side_effects=True, vmem_limit_bytes=60 * 2**20
        ),
    )(
        tokens, norm_gain[None], state_in_weight, pool_in_weight, rate_real, rate_imag, log_step[None],
        jnp.swapaxes(input_real, 1, 2), jnp.swapaxes(input_imag, 1, 2), output_real, output_imag,
        skip_gain[None], pool_weight, pool_gain[None], state_out_weight, pool_out_weight,
    )


def solution(mesh):
    n_sp, n_tp = mesh.shape["sp"], mesh.shape["tp"]
    n_x = 2 ** ((n_sp.bit_length() - 1) // 2)
    both, whole = P("sp", "tp"), P()
    return jax.shard_map(
        functools.partial(body, n_sp, n_tp, n_x),
        mesh=mesh,
        in_specs=(both, whole, both, both) + (whole,) * 10 + (both, both),
        out_specs=both,
        check_vma=False,
    )
```

profile of v0, /device:TPU:17, one launch (start us, length us, event | category | flops | bytes accessed | tf_op | source)
XLA Modules:
  0.0 76.0 jit_solution(1755389296602537847)
XLA Ops:
  0.0 74.2 %shard_map.154 = bf16[256,768]{1,0:T(8,128)(2,1)} custom-call(bf16[256,768]{1,0:T(8,128)(2,1)} %tok_ref.1, f32[1,3072]{1,0:T(1,128)} %bitcast.8, bf16[384,256]{1,0:T(8,128)(2,1)} %wsi_ref.1, bf16[384,256]{1,0:T(8,128)(2,1)} %wpi_ref.1, f32[64,64]{1,0:T(8,128)} %rr_ref.1, f32[64,64]{1,0:T(8,128)} %ri_ref.1, f32[1,64]{1,0:T(1,128)} %bitcast.11, ...), custom_call_target="tpu_custom_call" | custom-call | tf_op jit(solution)/shard_map/pallas_call | solution.py:469
  74.2 1.8 %copy.18 = bf16[256,768]{1,0:T(8,128)(2,1)} copy(bf16[256,768]{1,0:T(8,128)(2,1)} %shard_map.154) | data formatting | bytes 786432
where the time goes:
time: 77 us; the launch traced here: 76 us
  Pallas kernels  74.2 us (96%)
  local copies, waits for them, and re-layouts  1.77 us (2%)
    pallas_call x1, Pallas kernels, body(): pl.pallas_call(functools.partial(kernel, n_sp, n_tp, n_x, states), out_sh...  74.2 us
    unnamed x1, local copies, waits for them, and re-layouts  1.77 us

commit v1 on v0

--- a/solution.py
+++ b/solution.py
@@ -448,6 +448,648 @@
     for k in range(1, n_sp):
         end_copy(k).wait_send()
 
+LANES = 128
+HALVES = 2
+
+
+def slab_kernel(
+    n_sp, n_tp, n_x, states,
+    tok_ref, gain_ref, wsi_ref, wpi_ref, rr_ref, ri_ref, step_ref, inr_ref, ini_ref, outr_ref,
+    outi_ref, skip_ref, pw_ref, pg_ref, wso_ref, wpo_ref,
+    out_ref,
+    tok, scaled, squares, w_in, w_out, dmat, rmat, pmat, push, order, halo, halo_out, ends, act,
+    mine_s, mine_p, made, outx, rates, matrices, pool_own, dec_ref,
+    own_sem, xw_send, xw_recv, z_send, z_recv, tok_send, tok_recv, act_send, act_recv, halo_sem, end_send, end_recv,
+    out_send, out_recv,
+):
+    me, tp = lax.axis_index("sp"), lax.axis_index("tp")
+    n_z = n_sp // n_x
+    z, x = me // n_x, me % n_x
+    y, core = tp // 2, tp % 2
+    rows = tok_ref.shape[0]
+    slab = rows * n_x
+    features = tok_ref.shape[1]
+    in_rows = wsi_ref.shape[0]
+    out_rows = wso_ref.shape[0]
+    width = wsi_ref.shape[1] // n_x
+    out_width = wso_ref.shape[1] // n_x
+    chunk_count = out_width // LANES
+    groups = width // SSM_GROUP
+    columns = groups * states
+    pool_groups = width // POOL_GROUP
+    span = slab // CHUNKS
+    q = tp * n_x + x
+
+    across, pair, both = (1 - y) * 2 + core, y * 2 + 1 - core, (1 - y) * 2 + 1 - core
+    beside = me + 1 - 2 * x
+    to_x, to_y, to_pair = (beside, tp), (me, across), (me, pair)
+    ways = (1, -1)
+
+    def to_z(way):
+        return (me + way * n_x, tp)
+
+    def inside(at):
+        return jnp.logical_and(at >= 0, at < n_z)
+
+    def aligned(index, size):
+        return pl.ds(pl.multiple_of(index * size, size), size)
+
+    barrier = pltpu.get_barrier_semaphore()
+    for there in (to_x, to_y, to_pair):
+        pl.semaphore_signal(barrier, inc=1, device_id=there, device_id_type=MESH)
+    for way in ways:
+        @pl.when(inside(z + way))
+        def _():
+            pl.semaphore_signal(barrier, inc=1, device_id=to_z(way), device_id_type=MESH)
+
+    def remote(source, there, send, recv, target):
+        return pltpu.make_async_remote_copy(
+            source, there, send, recv, device_id=target, device_id_type=MESH
+        )
+
+    def in_part(ref, half):
+        return ref.at[:, aligned(half, width)]
+
+    def out_part(ref, half, j):
+        return ref.at[:, pl.ds(pl.multiple_of(half * out_width + j * LANES, LANES), LANES)]
+
+    own_in, own_out = (wsi_ref, wpi_ref), (wso_ref, wpo_ref)
+
+    def in_at(m, sp):
+        return w_in.at[m, aligned(sp, in_rows)]
+
+    def out_at(j, m, sp):
+        return w_out.at[j, m, aligned(sp, out_rows)]
+
+    own_copies = [pltpu.make_async_copy(in_part(own_in[m], x), in_at(m, me), own_sem.at[m]) for m in range(2)]
+    for j in range(chunk_count):
+        for m in range(2):
+            own_copies.append(
+                pltpu.make_async_copy(out_part(own_out[m], x, j), out_at(j, m, me), own_sem.at[2 + 2 * j + m])
+            )
+    base = 2 + 2 * chunk_count
+    tok_copy = pltpu.make_async_copy(tok_ref, tok.at[tp, aligned(x, rows)], own_sem.at[base])
+
+    def heads(ref, count):
+        return ref.at[aligned(q, count)]
+
+    loads = [
+        pltpu.make_async_copy(heads(ref, groups), there, own_sem.at[base + 1 + k])
+        for k, (ref, there) in enumerate(
+            (
+                (rr_ref, rates.at[0]), (ri_ref, rates.at[1]), (inr_ref, matrices.at[0]),
+                (ini_ref, matrices.at[1]), (outr_ref, matrices.at[2]), (outi_ref, matrices.at[3]),
+            )
+        )
+    ]
+    loads.append(pltpu.make_async_copy(heads(pw_ref, pool_groups), pool_own, own_sem.at[base + 7]))
+    for c in loads + [tok_copy] + own_copies:
+        c.start()
+
+    def x_weights(k, sp):
+        if k < 2:
+            return in_part(own_in[k], 1 - x), in_at(k, sp)
+        j, m = (k - 2) // 2, k % 2
+        return out_part(own_out[m], 1 - x, j), out_at(j, m, sp)
+
+    def x_send(k):
+        return remote(*x_weights(k, me), xw_send.at[k], xw_recv.at[k], to_x)
+
+    @jax.named_scope("across_wait")
+    def x_wait(k):
+        here = x_weights(k, beside)[1]
+        remote(here, here, xw_send.at[k], xw_recv.at[k], to_x).wait_recv()
+
+    x_kinds = 2 + 2 * chunk_count
+    stage_count = 2 + chunk_count
+
+    def z_part(stage, h, at):
+        if stage < 2:
+            return in_at(stage, at * n_x + (x if h == 0 else 1 - x))
+        return w_out.at[stage - 2, h, aligned(at, out_rows * n_x)]
+
+    def z_copy(d, stage, s, h):
+        there = z_part(stage, h, z - ways[d] * s)
+        source = in_part(own_in[stage], x) if s == 0 and stage < 2 and h == 0 else there
+        return remote(source, there, z_send.at[d, stage, s, h], z_recv.at[d, stage, s, h], to_z(ways[d]))
+
+    def z_own(stage, h):
+        for d in range(2):
+            @pl.when(inside(z + ways[d]))
+            def _():
+                z_copy(d, stage, 0, h).start()
+
+    def middle():
+        return jnp.logical_and(inside(z + 1), inside(z - 1))
+
+    def z_arrive(d, stage, s, h):
+        here = z_part(stage, h, z - ways[d] * (s + 1))
+        remote(here, here, z_send.at[d, stage, s, h], z_recv.at[d, stage, s, h], to_z(ways[d])).wait_recv()
+
+    @jax.named_scope("relay_wait")
+    def z_relay(stage, s, h):
+        for d in range(2):
+            @pl.when(jnp.logical_and(inside(z - ways[d] * (s + 1)), inside(z + ways[d])))
+            def _():
+                z_arrive(d, stage, s, h)
+                z_copy(d, stage, s + 1, h).start()
+
+    @jax.named_scope("final_wait")
+    def z_final(stage):
+        for d in range(2):
+            for s in range(n_z - 1):
+                @pl.when(jnp.logical_and(inside(z - ways[d] * (s + 1)), jnp.logical_not(inside(z + ways[d]))))
+                def _():
+                    for h in range(2):
+                        z_arrive(d, stage, s, h)
+
+    def out_own(j):
+        for m in range(2):
+            x_wait(2 + 2 * j + m)
+            own_copies[2 + 2 * j + m].wait()
+            z_own(2 + j, m)
+
+    relays = [(m, 0, h) for h in range(2) for m in range(2)]
+    relays += [(m, s, h) for m in range(2) for s in range(1, n_z - 2) for h in range(2)]
+    in_relays = len(relays)
+    for j in range(chunk_count):
+        relays += [(2 + j, s, m) for s in range(n_z - 2) for m in range(2)]
+    turn = [0]
+
+    def progress(count=1, stop=None):
+        while count and turn[0] < (len(relays) if stop is None else stop):
+            z_relay(*relays[turn[0]])
+            turn[0] += 1
+            count -= 1
+
+    class Gather:
+        def __init__(self, own, region, send, recv):
+            self.own, self.region, self.send, self.recv = own, region, send, recv
+
+        def copy(self, slot, p):
+            region = self.region
+            source, there, target = {
+                0: (self.own(p), region(tp, x, p), to_x),
+                1: (self.own(p), region(tp, x, p), to_y),
+                2: (None, region(tp, 1 - x, p), to_y),
+                3: (self.own(p), region(tp, x, p), to_pair),
+                4: (None, region(tp, 1 - x, p), to_pair),
+                5: (None, region(across, x, p), to_pair),
+                6: (None, region(across, 1 - x, p), to_pair),
+            }[slot]
+            source = there if source is None else source
+            return remote(source, there, self.send.at[slot, p], self.recv.at[slot, p], target)
+
+        def start(self, *slots, p):
+            for slot in slots:
+                self.copy(slot, p).start()
+
+        @jax.named_scope("gather_wait")
+        def wait(self, slot, p):
+            at_tp, at_x = (
+                (tp, 1 - x), (across, x), (across, 1 - x), (pair, x), (pair, 1 - x), (both, x), (both, 1 - x)
+            )[slot]
+            here = self.region(at_tp, at_x, p)
+            remote(here, here, self.send.at[slot, p], self.recv.at[slot, p], to_pair).wait_recv()
+
+        def relay_x(self, p):
+            self.wait(0, p)
+            self.start(2, 4, p=p)
+
+        def relay_y(self, p):
+            self.wait(1, p)
+            self.start(5, p=p)
+
+        def relay_both(self, p):
+            self.wait(2, p)
+            self.start(6, p=p)
+
+        def drain(self):
+            for slot in range(7):
+                for p in range(HALVES):
+                    self.copy(slot, p).wait_send()
+
+    piece = rows // HALVES
+
+    def tok_region(at_tp, at_x, p):
+        return tok.at[at_tp, pl.ds(pl.multiple_of(at_x * rows + p * piece, piece), piece)]
+
+    tokens = Gather(lambda p: tok_ref.at[pl.ds(p * piece, piece)], tok_region, tok_send, tok_recv)
+
+    def act_gather(which, mine):
+        size = slab // HALVES
+
+        def region(at_tp, at_x, p):
+            return act.at[which, pl.ds(p * size, size), aligned(at_tp * n_x + at_x, width)]
+
+        return Gather(lambda p: mine.at[pl.ds(p * size, size)], region, act_send.at[which], act_recv.at[which])
+
+    acts = (act_gather(0, mine_s), act_gather(1, mine_p))
+
+    pl.semaphore_wait(barrier, 3 + inside(z + 1).astype(jnp.int32) + inside(z - 1).astype(jnp.int32))
+
+    x_send(0).start()
+    z_own(0, 0)
+    z_own(1, 0)
+    x_send(1).start()
+    for p in range(HALVES):
+        tokens.start(0, 1, 3, p=p)
+    for k in range(2, x_kinds):
+        x_send(k).start()
+
+    tile = iota((states, columns), 0) == iota((states, columns), 1) % states
+    tile_exact, tile_half = tile.astype(f32), tile.astype(bf16)
+
+    def exactly(a, b):
+        return jnp.dot(a, b, precision=lax.Precision.HIGHEST, preferred_element_type=f32)
+
+    factors = []
+
+    @jax.named_scope("build_decay")
+    def build_decay():
+        for c in loads:
+            c.wait()
+        own_head = iota((groups, columns), 0) == iota((groups, columns), 1) // states
+
+        def flat(a):
+            return jnp.sum(jnp.where(own_head, exactly(a, tile_exact), 0.0), axis=0, keepdims=True)
+
+        rate_real, rate_imag = flat(rates[0]), flat(rates[1])
+        all_groups = step_ref.shape[1]
+        head = iota((all_groups, columns), 0) == q * groups + iota((all_groups, columns), 1) // states
+        log_step = exactly(jnp.broadcast_to(step_ref[...], (8, all_groups)), head.astype(f32))[0:1]
+        step_size = jnp.exp(log_step) / (rows * n_sp)
+        exponent, angle = rate_real * step_size, rate_imag * step_size
+        magnitude = jnp.exp(exponent)
+        cosine = jnp.cos(angle)
+        decay_real, decay_imag = magnitude * cosine, magnitude * jnp.sin(angle)
+        series = jnp.ones_like(exponent)
+        for k in range(10, 1, -1):
+            series = 1.0 + series * exponent * (1.0 / k)
+        growth = jnp.where(jnp.abs(exponent) < 0.5, exponent * series, magnitude - 1.0)
+        less_one = growth * cosine - 2.0 * jnp.square(jnp.sin(0.5 * angle))
+        denominator = rate_real * rate_real + rate_imag * rate_imag
+        factors.append((less_one * rate_real + decay_imag * rate_imag) / denominator)
+        factors.append((decay_imag * rate_real - less_one * rate_imag) / denominator)
+        dec_ref[0:1, :] = decay_real
+        dec_ref[1:2, :] = decay_imag
+
+    def spread(k):
+        high, low = split(matrices[k].reshape(width, states))
+        return dot(high, tile_half) + dot(low, tile_half)
+
+    @jax.named_scope("build_drive")
+    def build_drive(i):
+        same = iota((width, columns), 0) // SSM_GROUP == iota((width, columns), 1) // states
+        real, imag = spread(0), spread(1)
+        if i == 0:
+            drive = factors[0] * real - factors[1] * imag
+        else:
+            drive = factors[0] * imag + factors[1] * real
+        for j, part in enumerate(split(jnp.where(same, drive, 0.0))):
+            dmat[i, j] = part
+
+    @jax.named_scope("build_read")
+    def build_read(i):
+        onto = (iota((columns, states), 0) % states == iota((columns, states), 1)).astype(bf16)
+        same = iota((columns, width), 0) // states == iota((columns, width), 1) // SSM_GROUP
+        for j, part in enumerate(split(matrices[2 + i].reshape(width, states))):
+            rmat[i, j] = jnp.where(same, dot_nt(onto, part), 0.0).astype(bf16)
+
+    @jax.named_scope("build_pool")
+    def build_pool():
+        onto = (iota((POOL_GROUP, width), 0) == iota((POOL_GROUP, width), 1) % POOL_GROUP).astype(bf16)
+        same = iota((width, width), 0) // POOL_GROUP == iota((width, width), 1) // POOL_GROUP
+        own = pool_own[...].reshape(width, POOL_GROUP)
+        pmat[...] = jnp.where(same, dot(own, onto), 0.0).astype(bf16)
+
+    @jax.named_scope("build_order")
+    def build_order(i):
+        a, b = iota((slab, slab), i), iota((slab, slab), 1 - i)
+        order[i] = (b == (a % CHUNKS) * span + a // CHUNKS).astype(bf16)
+
+    @jax.named_scope("take")
+    def take(at_tp, first):
+        cut = pl.ds(pl.multiple_of(at_tp * features, features), features)
+        gain = gain_ref[:, cut]
+        size = min(64, slab)
+
+        def step(i, _):
+            here = pl.ds(pl.multiple_of(i * size, size), size)
+            block = tok[at_tp, here].astype(f32)
+            total = jnp.broadcast_to(jnp.sum(block * block, axis=1, keepdims=True), (size, LANES))
+            squares[here] = total if first else squares[here] + total
+            scaled[here, cut] = (block * gain).astype(bf16)
+            return 0
+
+        lax.fori_loop(0, slab // size, step, 0)
+
+    build_decay()
+    build_drive(0)
+    progress()
+    x_wait(0)
+    z_own(0, 1)
+    progress()
+    x_wait(1)
+    z_own(1, 1)
+    build_drive(1)
+    build_read(0)
+    progress()
+    build_read(1)
+    progress()
+    tokens.relay_x(0)
+    build_order(0)
+    progress()
+    build_pool()
+    tokens.relay_y(0)
+    tokens.relay_x(1)
+    progress()
+    tok_copy.wait()
+    build_order(1)
+    progress(stop=in_relays)
+    tokens.relay_y(1)
+    for p in range(HALVES):
+        tokens.wait(3, p)
+        tokens.wait(4, p)
+    take(tp, True)
+    progress(stop=in_relays)
+    take(pair, False)
+    tokens.relay_both(0)
+    progress(stop=in_relays)
+    tokens.relay_both(1)
+    take(across, False)
+    for p in range(HALVES):
+        tokens.wait(5, p)
+        tokens.wait(6, p)
+    take(both, False)
+    progress(in_relays, stop=in_relays)
+    inverse = lax.rsqrt(squares[...] / (features * n_tp) + epsilon)
+    own_copies[0].wait()
+    z_final(0)
+    state_in = (dot(scaled[...], w_in[0]) * inverse).astype(bf16)
+    out_own(0)
+    signal = dot(order[0], state_in).astype(bf16)
+    for i in range(2):
+        push[i] = dot(signal, dmat[i, 0]) + dot(signal, dmat[i, 1])
+    decay_real = jnp.broadcast_to(dec_ref[0:1, :], (CHUNKS, columns))
+    decay_imag = jnp.broadcast_to(dec_ref[1:2, :], (CHUNKS, columns))
+
+    def advance(p, carry):
+        cut = pl.ds(pl.multiple_of(p * CHUNKS, CHUNKS), CHUNKS)
+        real, imag = cmul(decay_real, decay_imag, *carry)
+        real, imag = real + push[0, cut, :], imag + push[1, cut, :]
+        push[0, cut, :] = real
+        push[1, cut, :] = imag
+        return real, imag
+
+    zero = jnp.zeros((CHUNKS, columns), f32)
+    end_real, end_imag = lax.fori_loop(0, span, advance, (zero, zero), unroll=4)
+
+    def power(real, imag, count):
+        out = None
+        while count:
+            if count % 2:
+                out = (real, imag) if out is None else cmul(*out, real, imag)
+            real, imag = cmul(real, imag, real, imag)
+            count //= 2
+        return out
+
+    chunk_decay = power(dec_ref[0:1, :], dec_ref[1:2, :], span)
+    block_decay = power(*chunk_decay, CHUNKS)
+    row_zero = jnp.zeros((1, columns), f32)
+    total = (row_zero, row_zero)
+    for j in range(CHUNKS):
+        moved = cmul(*chunk_decay, *total)
+        total = (moved[0] + end_real[j : j + 1], moved[1] + end_imag[j : j + 1])
+    which = iota((CHUNKS, columns), 0)
+    ends[z] = jnp.where(which == 0, total[0], jnp.where(which == 1, total[1], 0.0))
+
+    def end_copy(k):
+        return remote(ends.at[z], ends.at[z], end_send.at[k - 1], end_recv.at[k - 1], (me + k * n_x, tp))
+
+    for k in range(1, n_z):
+        @pl.when(inside(z + k))
+        def _():
+            end_copy(k).start()
+
+    out_own(1)
+    progress()
+    z_final(1)
+    own_copies[1].wait()
+    pool_in = (dot(scaled[...], w_in[1]) * inverse).astype(bf16)
+    halo_out[...] = pool_in[slab - window_reach :]
+    halo_copy = remote(halo_out, halo, halo_sem.at[0], halo_sem.at[1], to_z(1))
+
+    @pl.when(inside(z + 1))
+    def _():
+        halo_copy.start()
+
+    progress()
+    for k in range(1, n_z):
+        @pl.when(inside(z - k))
+        @jax.named_scope("ends_wait")
+        def _():
+            there = ends.at[z - k]
+            remote(there, there, end_send.at[k - 1], end_recv.at[k - 1], to_z(1)).wait_recv()
+
+    total = (row_zero, row_zero)
+    for s in range(n_z - 1):
+        moved = cmul(*block_decay, *total)
+        use = s < z
+        total = (
+            jnp.where(use, moved[0] + ends[s, 0:1, :], total[0]),
+            jnp.where(use, moved[1] + ends[s, 1:2, :], total[1]),
+        )
+    begin_real, begin_imag = zero, zero
+    for j in range(CHUNKS):
+        begin_real = jnp.where(which == j, total[0], begin_real)
+        begin_imag = jnp.where(which == j, total[1], begin_imag)
+        moved = cmul(*chunk_decay, *total)
+        total = (moved[0] + end_real[j : j + 1], moved[1] + end_imag[j : j + 1])
+
+    def add_carry(p, carry):
+        cut = pl.ds(pl.multiple_of(p * CHUNKS, CHUNKS), CHUNKS)
+        real, imag = cmul(decay_real, decay_imag, *carry)
+        push[0, cut, :] = push[0, cut, :] + real
+        push[1, cut, :] = push[1, cut, :] + imag
+        return real, imag
+
+    lax.fori_loop(0, span, add_carry, (begin_real, begin_imag), unroll=4)
+    progress()
+    real_high, real_low = split(push[0])
+    imag_high, imag_low = split(push[1])
+    readout = dot(real_high, rmat[0, 0]) + dot(real_high, rmat[0, 1]) + dot(real_low, rmat[0, 0])
+    readout -= dot(imag_high, rmat[1, 0]) + dot(imag_high, rmat[1, 1]) + dot(imag_low, rmat[1, 0])
+    skip = skip_ref[:, aligned(q, width)]
+    readout += skip * signal.astype(f32)
+    shuffled = jax.nn.gelu(readout).astype(bf16)
+    mine_s[...] = dot(order[1], shuffled).astype(bf16)
+    for p in range(HALVES):
+        acts[0].start(0, 1, 3, p=p)
+    act[0, :, aligned(q, width)] = mine_s[...]
+    out_own(2) if chunk_count > 2 else None
+    progress()
+
+    @pl.when(z > 0)
+    @jax.named_scope("halo_wait")
+    def _():
+        halo_copy.wait_recv()
+
+    before = jnp.where(z == 0, jnp.zeros_like(halo), halo[...])
+    whole = jnp.concatenate([before, pool_in], axis=0).astype(f32)
+    window = jnp.left_shift(2, (q * pool_groups + iota((slab, width), 1) // POOL_GROUP) % 4)
+    sums = jnp.zeros((slab, width), f32)
+    running = whole
+    for level in range(4):
+        running = running + pltpu.roll(running, 2**level, 0)
+        sums = jnp.where(window == 2 ** (level + 1), running[window_reach:], sums)
+    position = z * slab + iota((slab, width), 0)
+    divisor = jnp.minimum(position + 1, window).astype(f32)
+    pooled = sums / divisor - whole[window_reach:]
+    pooled_high, pooled_low = split(pooled)
+    pool_gain = pg_ref[:, aligned(q, width)]
+    projected = dot(pooled_high, pmat[...]) + dot(pooled_low, pmat[...])
+    mine_p[...] = (projected * pool_gain).astype(bf16)
+    for p in range(HALVES):
+        acts[1].start(0, 1, 3, p=p)
+    act[1, :, aligned(q, width)] = mine_p[...]
+    for k in range(2):
+        for p in range(HALVES):
+            acts[k].relay_x(p)
+            progress()
+            acts[k].relay_y(p)
+        progress()
+    for k in range(2):
+        for p in range(HALVES):
+            acts[k].relay_both(p)
+            progress()
+    progress(len(relays))
+    for k in range(2):
+        for slot in (3, 4, 5, 6):
+            for p in range(HALVES):
+                acts[k].wait(slot, p)
+
+    def out_copy(j):
+        return remote(made.at[j, aligned(1 - x, rows)], outx.at[j], out_send.at[j], out_recv.at[j], to_x)
+
+    def out_columns(half, j):
+        return pl.ds(pl.multiple_of(half * out_width + j * LANES, LANES), LANES)
+
+    def keep(j):
+        return pltpu.make_async_copy(made.at[j, aligned(x, rows)], out_ref.at[:, out_columns(x, j)], own_sem.at[base + 8 + j])
+
+    def fetch(j):
+        return pltpu.make_async_copy(outx.at[j], out_ref.at[:, out_columns(1 - x, j)], own_sem.at[base + 8 + chunk_count + j])
+
+    def make(j, half):
+        cut = aligned(half, rows)
+        made[j, cut] = (dot(act[0, cut], w_out[j, 0]) + dot(act[1, cut], w_out[j, 1])).astype(bf16)
+
+    for j in range(chunk_count):
+        z_final(2 + j)
+        make(j, 1 - x)
+        out_copy(j).start()
+        make(j, x)
+        keep(j).start()
+
+    for k in range(x_kinds):
+        x_send(k).wait_send()
+    for d in range(2):
+        for stage in range(stage_count):
+            for s in range(n_z - 1):
+                @pl.when(jnp.logical_and(inside(z + ways[d]), inside(z - ways[d] * s)))
+                def _():
+                    for h in range(2):
+                        z_copy(d, stage, s, h).wait_send()
+    tokens.drain()
+    acts[0].drain()
+    acts[1].drain()
+
+    @pl.when(inside(z + 1))
+    def _():
+        halo_copy.wait_send()
+
+    for k in range(1, n_z):
+        @pl.when(inside(z + k))
+        def _():
+            end_copy(k).wait_send()
+    for j in range(chunk_count):
+        out_copy(j).wait_recv()
+        fetch(j).start()
+    for j in range(chunk_count):
+        out_copy(j).wait_send()
+        keep(j).wait()
+        fetch(j).wait()
+
+
+def slab_call(n_sp, n_tp, n_x, arrays):
+    tokens, state_in_weight, state_out_weight = arrays[0], arrays[2], arrays[14]
+    rows, features = tokens.shape
+    in_rows, width = state_in_weight.shape
+    out_rows, out_columns = state_out_weight.shape
+    width //= n_x
+    n_z, slab, chunk_count = n_sp // n_x, rows * n_x, out_columns // n_x // LANES
+    groups, states = width // SSM_GROUP, arrays[4].shape[1]
+    columns, pool_groups = groups * states, width // POOL_GROUP
+    vmem = pl.BlockSpec(memory_space=pltpu.VMEM)
+    anywhere = pl.BlockSpec(memory_space=pl.ANY)
+    dma = pltpu.SemaphoreType.DMA
+    return pl.pallas_call(
+        functools.partial(slab_kernel, n_sp, n_tp, n_x, states),
+        out_shape=jax.ShapeDtypeStruct((rows, out_columns), bf16),
+        in_specs=[anywhere, vmem] + [anywhere] * 4 + [vmem] + [anywhere] * 4 + [vmem, anywhere, vmem]
+        + [anywhere] * 2,
+        out_specs=anywhere,
+        scratch_shapes=[
+            pltpu.VMEM((n_tp, slab, features), bf16),
+            pltpu.VMEM((slab, features * n_tp), bf16),
+            pltpu.VMEM((slab, LANES), f32),
+            pltpu.VMEM((2, n_sp * in_rows, width), bf16),
+            pltpu.VMEM((chunk_count, 2, n_sp * out_rows, LANES), bf16),
+            pltpu.VMEM((2, 2, width, columns), bf16),
+            pltpu.VMEM((2, 2, columns, width), bf16),
+            pltpu.VMEM((width, width), bf16),
+            pltpu.VMEM((2, slab, columns), f32),
+            pltpu.VMEM((2, slab, slab), bf16),
+            pltpu.VMEM((window_reach, width), bf16),
+            pltpu.VMEM((window_reach, width), bf16),
+            pltpu.VMEM((n_z, CHUNKS, columns), f32),
+            pltpu.VMEM((2, slab, n_tp * n_x * width), bf16),
+            pltpu.VMEM((slab, width), bf16),
+            pltpu.VMEM((slab, width), bf16),
+            pltpu.VMEM((chunk_count, slab, LANES), bf16),
+            pltpu.VMEM((chunk_count, rows, LANES), bf16),
+            pltpu.VMEM((2, groups, states), f32),
+            pltpu.VMEM((4, groups, SSM_GROUP, states), f32),
+            pltpu.VMEM((pool_groups, POOL_GROUP, POOL_GROUP), bf16),
+            pltpu.VMEM((2, columns), f32),
+            dma((10 + 4 * chunk_count,)),
+            dma((2 + 2 * chunk_count,)),
+            dma((2 + 2 * chunk_count,)),
+            dma((2, 2 + chunk_count, n_z - 1, 2)),
+            dma((2, 2 + chunk_count, n_z - 1, 2)),
+            dma((7, HALVES)),
+            dma((7, HALVES)),
+            dma((2, 7, HALVES)),
+            dma((2, 7, HALVES)),
+            dma((2,)),
+            dma((n_z - 1,)),
+            dma((n_z - 1,)),
+            dma((chunk_count,)),
+            dma((chunk_count,)),
+        ],
+        compiler_params=pltpu.CompilerParams(
+            collective_id=0, has_side_effects=True, vmem_limit_bytes=60 * 2**20
+        ),
+    )(*arrays)
+
+
+def slab_fits(n_sp, n_tp, n_x, width, pool_width, out_columns):
+    return (
+        n_x == 2 and n_tp == 4 and n_sp // n_x >= 3 and width == n_x * LANES
+        and pool_width == width and out_columns % (n_x * LANES) == 0
+    )
+
 
 def body(
     n_sp, n_tp, n_x,
@@ -463,6 +1105,12 @@
     states = rate_real.shape[1]
     columns = groups * states
     pool_groups = pool_width // POOL_GROUP
+    if slab_fits(n_sp, n_tp, n_x, width, pool_width, out_columns):
+        return slab_call(n_sp, n_tp, n_x, (
+            tokens, norm_gain[None], state_in_weight, pool_in_weight, rate_real, rate_imag, log_step[None],
+            jnp.swapaxes(input_real, 1, 2), jnp.swapaxes(input_imag, 1, 2), output_real, output_imag,
+            skip_gain[None], pool_weight, pool_gain[None], state_out_weight, pool_out_weight,
+        ))
     vmem = pl.BlockSpec(memory_space=pltpu.VMEM)
     anywhere = pl.BlockSpec(memory_space=pl.ANY)
     dma = pltpu.SemaphoreType.DMA

time: 77 us -> 70.7 us (0.918)
  the two profiles are of different devices: /device:TPU:17 before, /device:TPU:0 now
where the time goes in v1:
time: 70.7 us; the launch traced here: 70.5 us
  Pallas kernels  68.7 us (97%)
  local copies, waits for them, and re-layouts  1.77 us (3%)
    pallas_call x1, Pallas kernels, slab_call(): pl.pallas_call(functools.partial(slab_kernel, n_sp, n_tp, n_x, states), o...  68.7 us
    unnamed x1, local copies, waits for them, and re-layouts  1.77 us

profile of v1, /device:TPU:0, one launch (start us, length us, event | category | flops | bytes accessed | tf_op | source)
XLA Modules:
  0.0 70.5 jit_solution(13626291872244573891)
XLA Ops:
  0.0 68.7 %shard_map.154 = bf16[256,768]{1,0:T(8,128)(2,1)} custom-call(bf16[256,768]{1,0:T(8,128)(2,1)} %tok_ref.1, f32[1,3072]{1,0:T(1,128)} %bitcast.8, bf16[384,256]{1,0:T(8,128)(2,1)} %wsi_ref.1, bf16[384,256]{1,0:T(8,128)(2,1)} %wpi_ref.1, f32[64,64]{1,0:T(8,128)} %rr_ref.1, f32[64,64]{1,0:T(8,128)} %ri_ref.1, f32[1,64]{1,0:T(1,128)} %bitcast.11, ...), custom_call_target="tpu_custom_call" | custom-call | tf_op jit(solution)/shard_map/pallas_call | solution.py:1037
  68.8 1.8 %copy.18 = bf16[256,768]{1,0:T(8,128)(2,1)} copy(bf16[256,768]{1,0:T(8,128)(2,1)} %shard_map.154) | data formatting | bytes 786432

commit v2 on v1

--- a/solution.py
+++ b/solution.py
@@ -458,7 +458,7 @@
     outi_ref, skip_ref, pw_ref, pg_ref, wso_ref, wpo_ref,
     out_ref,
     tok, scaled, squares, w_in, w_out, dmat, rmat, pmat, push, order, halo, halo_out, ends, act,
-    mine_s, mine_p, made, outx, rates, matrices, pool_own, dec_ref,
+    made, rates, matrices, pool_own, dec_ref,
     own_sem, xw_send, xw_recv, z_send, z_recv, tok_send, tok_recv, act_send, act_recv, halo_sem, end_send, end_recv,
     out_send, out_recv,
 ):
@@ -521,29 +521,34 @@
     def out_at(j, m, sp):
         return w_out.at[j, m, aligned(sp, out_rows)]
 
-    own_copies = [pltpu.make_async_copy(in_part(own_in[m], x), in_at(m, me), own_sem.at[m]) for m in range(2)]
-    for j in range(chunk_count):
-        for m in range(2):
-            own_copies.append(
-                pltpu.make_async_copy(out_part(own_out[m], x, j), out_at(j, m, me), own_sem.at[2 + 2 * j + m])
-            )
-    base = 2 + 2 * chunk_count
+    def own_copy(k):
+        if k < 2:
+            return [pltpu.make_async_copy(in_part(own_in[k], x), in_at(k, me), own_sem.at[k])]
+        return [
+            pltpu.make_async_copy(out_part(own_out[m], x, k - 2), out_at(k - 2, m, me), own_sem.at[k])
+            for m in range(2)
+        ]
+
+    def own_wait(k):
+        here = in_at(k, me) if k < 2 else w_out.at[k - 2, :, aligned(me, out_rows)]
+        pltpu.make_async_copy(here, here, own_sem.at[k]).wait()
+
+    base = 2 + chunk_count
     tok_copy = pltpu.make_async_copy(tok_ref, tok.at[tp, aligned(x, rows)], own_sem.at[base])
 
     def heads(ref, count):
         return ref.at[aligned(q, count)]
 
     loads = [
-        pltpu.make_async_copy(heads(ref, groups), there, own_sem.at[base + 1 + k])
-        for k, (ref, there) in enumerate(
-            (
-                (rr_ref, rates.at[0]), (ri_ref, rates.at[1]), (inr_ref, matrices.at[0]),
-                (ini_ref, matrices.at[1]), (outr_ref, matrices.at[2]), (outi_ref, matrices.at[3]),
-            )
+        pltpu.make_async_copy(heads(ref, count), there, own_sem.at[base + 1 + k])
+        for ref, count, there, k in (
+            (rr_ref, groups, rates.at[0], 0), (ri_ref, groups, rates.at[1], 0),
+            (inr_ref, groups, matrices.at[0], 1), (ini_ref, groups, matrices.at[1], 1),
+            (outr_ref, groups, matrices.at[2], 1), (outi_ref, groups, matrices.at[3], 1),
+            (pw_ref, pool_groups, pool_own, 2),
         )
     ]
-    loads.append(pltpu.make_async_copy(heads(pw_ref, pool_groups), pool_own, own_sem.at[base + 7]))
-    for c in loads + [tok_copy] + own_copies:
+    for c in own_copy(0) + [tok_copy] + loads + [c for k in range(1, base) for c in own_copy(k)]:
         c.start()
 
     def x_weights(k, sp):
@@ -552,15 +557,19 @@
         j, m = (k - 2) // 2, k % 2
         return out_part(own_out[m], 1 - x, j), out_at(j, m, sp)
 
+    x_kinds = 2 + 2 * chunk_count
+
+    def x_slot(k):
+        return xw_recv.at[k if k < 2 else 2 + (k - 2) // 2]
+
     def x_send(k):
-        return remote(*x_weights(k, me), xw_send.at[k], xw_recv.at[k], to_x)
+        return remote(*x_weights(k, me), xw_send.at[0], x_slot(k), to_x)
 
     @jax.named_scope("across_wait")
     def x_wait(k):
-        here = x_weights(k, beside)[1]
-        remote(here, here, xw_send.at[k], xw_recv.at[k], to_x).wait_recv()
-
-    x_kinds = 2 + 2 * chunk_count
+        here = in_at(k, beside) if k < 2 else w_out.at[k - 2, :, aligned(beside, out_rows)]
+        remote(here, here, xw_send.at[0], xw_recv.at[k], to_x).wait_recv()
+
     stage_count = 2 + chunk_count
 
     def z_part(stage, h, at):
@@ -569,9 +578,9 @@
         return w_out.at[stage - 2, h, aligned(at, out_rows * n_x)]
 
     def z_copy(d, stage, s, h):
-        there = z_part(stage, h, z - ways[d] * s)
-        source = in_part(own_in[stage], x) if s == 0 and stage < 2 and h == 0 else there
-        return remote(source, there, z_send.at[d, stage, s, h], z_recv.at[d, stage, s, h], to_z(ways[d]))
+        at = z - ways[d] * s
+        there = z_part(stage, h, at)
+        return remote(there, there, z_send.at[d, s], z_recv.at[stage, at, h], to_z(ways[d]))
 
     def z_own(stage, h):
         for d in range(2):
@@ -579,12 +588,10 @@
             def _():
                 z_copy(d, stage, 0, h).start()
 
-    def middle():
-        return jnp.logical_and(inside(z + 1), inside(z - 1))
-
     def z_arrive(d, stage, s, h):
-        here = z_part(stage, h, z - ways[d] * (s + 1))
-        remote(here, here, z_send.at[d, stage, s, h], z_recv.at[d, stage, s, h], to_z(ways[d])).wait_recv()
+        at = z - ways[d] * (s + 1)
+        here = z_part(stage, h, at)
+        remote(here, here, z_send.at[d, s], z_recv.at[stage, at, h], to_z(ways[d])).wait_recv()
 
     @jax.named_scope("relay_wait")
     def z_relay(stage, s, h):
@@ -595,25 +602,25 @@
                 z_copy(d, stage, s + 1, h).start()
 
     @jax.named_scope("final_wait")
-    def z_final(stage):
+    def z_final(stage, distances=range(n_z - 1)):
         for d in range(2):
-            for s in range(n_z - 1):
+            for s in distances:
                 @pl.when(jnp.logical_and(inside(z - ways[d] * (s + 1)), jnp.logical_not(inside(z + ways[d]))))
                 def _():
                     for h in range(2):
                         z_arrive(d, stage, s, h)
 
     def out_own(j):
+        x_wait(2 + j)
+        own_wait(2 + j)
         for m in range(2):
-            x_wait(2 + 2 * j + m)
-            own_copies[2 + 2 * j + m].wait()
             z_own(2 + j, m)
 
     relays = [(m, 0, h) for h in range(2) for m in range(2)]
     relays += [(m, s, h) for m in range(2) for s in range(1, n_z - 2) for h in range(2)]
     in_relays = len(relays)
-    for j in range(chunk_count):
-        relays += [(2 + j, s, m) for s in range(n_z - 2) for m in range(2)]
+    later = [(2 + j, s, m) for j in range(chunk_count) for s in range(n_z - 2) for m in range(2)]
+    relays += sorted(later, key=lambda r: (r[0] > 2, r[1], r[0], r[2]))
     turn = [0]
 
     def progress(count=1, stop=None):
@@ -623,22 +630,14 @@
             count -= 1
 
     class Gather:
-        def __init__(self, own, region, send, recv):
-            self.own, self.region, self.send, self.recv = own, region, send, recv
+        def __init__(self, region, pair_region, send, recv):
+            self.region, self.pair_region, self.send, self.recv = region, pair_region, send, recv
 
         def copy(self, slot, p):
-            region = self.region
-            source, there, target = {
-                0: (self.own(p), region(tp, x, p), to_x),
-                1: (self.own(p), region(tp, x, p), to_y),
-                2: (None, region(tp, 1 - x, p), to_y),
-                3: (self.own(p), region(tp, x, p), to_pair),
-                4: (None, region(tp, 1 - x, p), to_pair),
-                5: (None, region(across, x, p), to_pair),
-                6: (None, region(across, 1 - x, p), to_pair),
-            }[slot]
-            source = there if source is None else source
-            return remote(source, there, self.send.at[slot, p], self.recv.at[slot, p], target)
+            at_tp, at_x = ((tp, x), (tp, x), (tp, 1 - x), (tp, x), (tp, 1 - x), (across, x), (across, 1 - x))[slot]
+            here = self.region(at_tp, at_x, p)
+            recv = self.recv.at[2 * slot + p if slot < 3 else 6 if slot < 5 else 7]
+            return remote(here, here, self.send, recv, (to_x, to_y, to_y, to_pair, to_pair, to_pair, to_pair)[slot])
 
         def start(self, *slots, p):
             for slot in slots:
@@ -646,11 +645,13 @@
 
         @jax.named_scope("gather_wait")
         def wait(self, slot, p):
-            at_tp, at_x = (
-                (tp, 1 - x), (across, x), (across, 1 - x), (pair, x), (pair, 1 - x), (both, x), (both, 1 - x)
-            )[slot]
-            here = self.region(at_tp, at_x, p)
-            remote(here, here, self.send.at[slot, p], self.recv.at[slot, p], to_pair).wait_recv()
+            here = self.region(*((tp, 1 - x), (across, x), (across, 1 - x))[slot], p)
+            remote(here, here, self.send, self.recv.at[2 * slot + p], to_pair).wait_recv()
+
+        @jax.named_scope("pair_wait")
+        def wait_pair(self, at_tp, k):
+            here = self.pair_region(at_tp)
+            remote(here, here, self.send, self.recv.at[6 + k], to_pair).wait_recv()
 
         def relay_x(self, p):
             self.wait(0, p)
@@ -664,34 +665,38 @@
             self.wait(2, p)
             self.start(6, p=p)
 
-        def drain(self):
-            for slot in range(7):
-                for p in range(HALVES):
-                    self.copy(slot, p).wait_send()
+        def drain(self, sent):
+            remote(sent, sent, self.send, self.recv.at[0], to_pair).wait_send()
 
     piece = rows // HALVES
 
     def tok_region(at_tp, at_x, p):
         return tok.at[at_tp, pl.ds(pl.multiple_of(at_x * rows + p * piece, piece), piece)]
 
-    tokens = Gather(lambda p: tok_ref.at[pl.ds(p * piece, piece)], tok_region, tok_send, tok_recv)
-
-    def act_gather(which, mine):
+    tokens = Gather(tok_region, lambda at_tp: tok.at[at_tp], tok_send.at[0], tok_recv)
+
+    def act_gather(which):
         size = slab // HALVES
 
         def region(at_tp, at_x, p):
             return act.at[which, pl.ds(p * size, size), aligned(at_tp * n_x + at_x, width)]
 
-        return Gather(lambda p: mine.at[pl.ds(p * size, size)], region, act_send.at[which], act_recv.at[which])
-
-    acts = (act_gather(0, mine_s), act_gather(1, mine_p))
+        def pair_region(at_tp):
+            return act.at[which, :, aligned(at_tp, n_x * width)]
+
+        return Gather(region, pair_region, act_send.at[which], act_recv.at[which])
+
+    acts = (act_gather(0), act_gather(1))
 
     pl.semaphore_wait(barrier, 3 + inside(z + 1).astype(jnp.int32) + inside(z - 1).astype(jnp.int32))
 
     x_send(0).start()
+    own_wait(0)
     z_own(0, 0)
+    own_wait(1)
     z_own(1, 0)
     x_send(1).start()
+    tok_copy.wait()
     for p in range(HALVES):
         tokens.start(0, 1, 3, p=p)
     for k in range(2, x_kinds):
@@ -804,30 +809,24 @@
     tokens.relay_y(0)
     tokens.relay_x(1)
     progress()
-    tok_copy.wait()
     build_order(1)
     progress(stop=in_relays)
     tokens.relay_y(1)
-    for p in range(HALVES):
-        tokens.wait(3, p)
-        tokens.wait(4, p)
+    tokens.wait_pair(pair, 0)
     take(tp, True)
     progress(stop=in_relays)
     take(pair, False)
+    progress(stop=in_relays)
     tokens.relay_both(0)
-    progress(stop=in_relays)
+    out_own(0)
     tokens.relay_both(1)
     take(across, False)
-    for p in range(HALVES):
-        tokens.wait(5, p)
-        tokens.wait(6, p)
+    tokens.wait_pair(both, 1)
     take(both, False)
-    progress(in_relays, stop=in_relays)
+    progress(2)
     inverse = lax.rsqrt(squares[...] / (features * n_tp) + epsilon)
-    own_copies[0].wait()
     z_final(0)
     state_in = (dot(scaled[...], w_in[0]) * inverse).astype(bf16)
-    out_own(0)
     signal = dot(order[0], state_in).astype(bf16)
     for i in range(2):
         push[i] = dot(signal, dmat[i, 0]) + dot(signal, dmat[i, 1])
@@ -872,10 +871,9 @@
         def _():
             end_copy(k).start()
 
-    out_own(1)
-    progress()
+    if chunk_count > 1:
+        out_own(1)
     z_final(1)
-    own_copies[1].wait()
     pool_in = (dot(scaled[...], w_in[1]) * inverse).astype(bf16)
     halo_out[...] = pool_in[slab - window_reach :]
     halo_copy = remote(halo_out, halo, halo_sem.at[0], halo_sem.at[1], to_z(1))
@@ -884,7 +882,9 @@
     def _():
         halo_copy.start()
 
-    progress()
+    progress(2)
+    for j in range(2, chunk_count):
+        out_own(j)
     for k in range(1, n_z):
         @pl.when(inside(z - k))
         @jax.named_scope("ends_wait")
@@ -915,7 +915,7 @@
         return real, imag
 
     lax.fori_loop(0, span, add_carry, (begin_real, begin_imag), unroll=4)
-    progress()
+    progress(2)
     real_high, real_low = split(push[0])
     imag_high, imag_low = split(push[1])
     readout = dot(real_high, rmat[0, 0]) + dot(real_high, rmat[0, 1]) + dot(real_low, rmat[0, 0])
@@ -923,12 +923,10 @@
     skip = skip_ref[:, aligned(q, width)]
     readout += skip * signal.astype(f32)
     shuffled = jax.nn.gelu(readout).astype(bf16)
-    mine_s[...] = dot(order[1], shuffled).astype(bf16)
+    act[0, :, aligned(q, width)] = dot(order[1], shuffled).astype(bf16)
     for p in range(HALVES):
         acts[0].start(0, 1, 3, p=p)
-    act[0, :, aligned(q, width)] = mine_s[...]
-    out_own(2) if chunk_count > 2 else None
-    progress()
+    progress(2)
 
     @pl.when(z > 0)
     @jax.named_scope("halo_wait")
@@ -949,77 +947,84 @@
     pooled_high, pooled_low = split(pooled)
     pool_gain = pg_ref[:, aligned(q, width)]
     projected = dot(pooled_high, pmat[...]) + dot(pooled_low, pmat[...])
-    mine_p[...] = (projected * pool_gain).astype(bf16)
+    act[1, :, aligned(q, width)] = (projected * pool_gain).astype(bf16)
     for p in range(HALVES):
         acts[1].start(0, 1, 3, p=p)
-    act[1, :, aligned(q, width)] = mine_p[...]
+    progress(2)
     for k in range(2):
         for p in range(HALVES):
             acts[k].relay_x(p)
+            acts[k].relay_y(p)
             progress()
-            acts[k].relay_y(p)
-        progress()
     for k in range(2):
         for p in range(HALVES):
             acts[k].relay_both(p)
             progress()
     progress(len(relays))
     for k in range(2):
-        for slot in (3, 4, 5, 6):
-            for p in range(HALVES):
-                acts[k].wait(slot, p)
-
-    def out_copy(j):
-        return remote(made.at[j, aligned(1 - x, rows)], outx.at[j], out_send.at[j], out_recv.at[j], to_x)
+        acts[k].wait_pair(pair, 0)
+        acts[k].wait_pair(both, 1)
 
     def out_columns(half, j):
         return pl.ds(pl.multiple_of(half * out_width + j * LANES, LANES), LANES)
 
-    def keep(j):
-        return pltpu.make_async_copy(made.at[j, aligned(x, rows)], out_ref.at[:, out_columns(x, j)], own_sem.at[base + 8 + j])
-
-    def fetch(j):
-        return pltpu.make_async_copy(outx.at[j], out_ref.at[:, out_columns(1 - x, j)], own_sem.at[base + 8 + chunk_count + j])
+    def out_copy(j):
+        return remote(made.at[j], out_ref.at[:, out_columns(x, j)], out_send.at[0], out_recv.at[0], to_x)
+
+    def part(j, half, at):
+        cut, depth = aligned(half, rows), aligned(at, n_x * out_rows)
+        return dot(act[0, cut, depth], w_out[j, 0, depth]) + dot(act[1, cut, depth], w_out[j, 1, depth])
 
     def make(j, half):
         cut = aligned(half, rows)
-        made[j, cut] = (dot(act[0, cut], w_out[j, 0]) + dot(act[1, cut], w_out[j, 1])).astype(bf16)
+        return dot(act[0, cut], w_out[j, 0]) + dot(act[1, cut], w_out[j, 1])
 
     for j in range(chunk_count):
-        z_final(2 + j)
-        make(j, 1 - x)
-        out_copy(j).start()
-        make(j, x)
-        keep(j).start()
-
-    for k in range(x_kinds):
-        x_send(k).wait_send()
-    for d in range(2):
-        for stage in range(stage_count):
+        if j + 1 < chunk_count:
+            z_final(2 + j)
+            made[j] = make(j, 1 - x).astype(bf16)
+            out_copy(j).start()
+            out_ref[:, out_columns(x, j)] = make(j, x).astype(bf16)
+        else:
+            far = n_z - 1 - z
+            z_final(2 + j, range(n_z - 2))
+            sums = [
+                sum(part(j, half, (far + 1 + r) % n_z) for r in range(n_z - 1)) for half in (1 - x, x)
+            ]
+            z_final(2 + j, range(n_z - 2, n_z - 1))
+            made[j] = (sums[0] + part(j, 1 - x, far)).astype(bf16)
+            out_copy(j).start()
+            out_ref[:, out_columns(x, j)] = (sums[1] + part(j, x, far)).astype(bf16)
+
+    @jax.named_scope("drain")
+    def drain():
+        sent = w_in.at[0, pl.ds(0, 2 * in_rows + 2 * chunk_count * out_rows)]
+        remote(sent, sent, xw_send.at[0], xw_recv.at[0], to_x).wait_send()
+        sent = w_in.at[0, pl.ds(0, n_x * (2 * in_rows + 2 * chunk_count * out_rows))]
+        for d in range(2):
             for s in range(n_z - 1):
                 @pl.when(jnp.logical_and(inside(z + ways[d]), inside(z - ways[d] * s)))
                 def _():
-                    for h in range(2):
-                        z_copy(d, stage, s, h).wait_send()
-    tokens.drain()
-    acts[0].drain()
-    acts[1].drain()
-
-    @pl.when(inside(z + 1))
-    def _():
-        halo_copy.wait_send()
-
-    for k in range(1, n_z):
-        @pl.when(inside(z + k))
+                    remote(sent, sent, z_send.at[d, s], z_recv.at[0, 0, 0], to_z(ways[d])).wait_send()
+        tokens.drain(scaled.at[pl.ds(0, 7 * rows // n_tp)])
+        for k in range(2):
+            acts[k].drain(act.at[k, :, pl.ds(0, 7 * width)])
+
+        @pl.when(inside(z + 1))
         def _():
-            end_copy(k).wait_send()
-    for j in range(chunk_count):
-        out_copy(j).wait_recv()
-        fetch(j).start()
-    for j in range(chunk_count):
-        out_copy(j).wait_send()
-        keep(j).wait()
-        fetch(j).wait()
+            halo_copy.wait_send()
+
+        for k in range(1, n_z):
+            @pl.when(inside(z + k))
+            def _():
+                end_copy(k).wait_send()
+
+        remote(made, made, out_send.at[0], out_recv.at[0], to_x).wait_send()
+
+    drain()
+    with jax.named_scope("out_wait"):
+        here = out_ref.at[:, aligned(1 - x, out_width)]
+        remote(here, here, out_send.at[0], out_recv.at[0], to_x).wait_recv()
 
 
 def slab_call(n_sp, n_tp, n_x, arrays):
@@ -1036,10 +1041,10 @@
     dma = pltpu.SemaphoreType.DMA
     return pl.pallas_call(
         functools.partial(slab_kernel, n_sp, n_tp, n_x, states),
-        out_shape=jax.ShapeDtypeStruct((rows, out_columns), bf16),
+        out_shape=pltpu.VMEM((rows, out_columns), bf16),
         in_specs=[anywhere, vmem] + [anywhere] * 4 + [vmem] + [anywhere] * 4 + [vmem, anywhere, vmem]
         + [anywhere] * 2,
-        out_specs=anywhere,
+        out_specs=vmem,
         scratch_shapes=[
             pltpu.VMEM((n_tp, slab, features), bf16),
             pltpu.VMEM((slab, features * n_tp), bf16),
@@ -1055,28 +1060,25 @@
             pltpu.VMEM((window_reach, width), bf16),
             pltpu.VMEM((n_z, CHUNKS, columns), f32),
             pltpu.VMEM((2, slab, n_tp * n_x * width), bf16),
-            pltpu.VMEM((slab, width), bf16),
-            pltpu.VMEM((slab, width), bf16),
-            pltpu.VMEM((chunk_count, slab, LANES), bf16),
             pltpu.VMEM((chunk_count, rows, LANES), bf16),
             pltpu.VMEM((2, groups, states), f32),
             pltpu.VMEM((4, groups, SSM_GROUP, states), f32),
             pltpu.VMEM((pool_groups, POOL_GROUP, POOL_GROUP), bf16),
             pltpu.VMEM((2, columns), f32),
-            dma((10 + 4 * chunk_count,)),
-            dma((2 + 2 * chunk_count,)),
-            dma((2 + 2 * chunk_count,)),
-            dma((2, 2 + chunk_count, n_z - 1, 2)),
-            dma((2, 2 + chunk_count, n_z - 1, 2)),
-            dma((7, HALVES)),
-            dma((7, HALVES)),
-            dma((2, 7, HALVES)),
-            dma((2, 7, HALVES)),
+            dma((6 + chunk_count,)),
+            dma((1,)),
+            dma((2 + chunk_count,)),
+            dma((2, n_z - 1)),
+            dma((2 + chunk_count, n_z, 2)),
+            dma((1,)),
+            dma((8,)),
+            dma((2,)),
+            dma((2, 8)),
             dma((2,)),
             dma((n_z - 1,)),
             dma((n_z - 1,)),
-            dma((chunk_count,)),
-            dma((chunk_count,)),
+            dma((1,)),
+            dma((1,)),
         ],
         compiler_params=pltpu.CompilerParams(
             collective_id=0, has_side_effects=True, vmem_limit_bytes=60 * 2**20
@@ -1084,10 +1086,11 @@
     )(*arrays)
 
 
-def slab_fits(n_sp, n_tp, n_x, width, pool_width, out_columns):
+def slab_fits(n_sp, n_tp, n_x, in_rows, width, pool_width, out_rows, out_columns):
     return (
         n_x == 2 and n_tp == 4 and n_sp // n_x >= 3 and width == n_x * LANES
         and pool_width == width and out_columns % (n_x * LANES) == 0
+        and n_x * (2 * in_rows + out_columns // (n_x * LANES) * 2 * out_rows) <= n_sp * in_rows
     )
 
 
@@ -1105,7 +1108,7 @@
     states = rate_real.shape[1]
     columns = groups * states
     pool_groups = pool_width // POOL_GROUP
-    if slab_fits(n_sp, n_tp, n_x, width, pool_width, out_columns):
+    if slab_fits(n_sp, n_tp, n_x, in_rows, width, pool_width, out_rows, out_columns):
         return slab_call(n_sp, n_tp, n_x, (
             tokens, norm_gain[None], state_in_weight, pool_in_weight, rate_real, rate_imag, log_step[None],
             jnp.swapaxes(input_real, 1, 2), jnp.swapaxes(input_imag, 1, 2), output_real, output_imag,

time: 70.7 us -> 62.1 us (0.88)
  the two profiles are of different devices: /device:TPU:0 before, /device:TPU:17 now
where the time goes in v2:
time: 62.1 us; the launch traced here: 61.1 us
  Pallas kernels  60.3 us (97%)
  local copies, waits for them, and re-layouts  0.75 us (1%)
    pallas_call x1, Pallas kernels, slab_call(): pl.pallas_call(functools.partial(slab_kernel, n_sp, n_tp, n_x, states), o...  60.3 us

profile of v2, /device:TPU:17, one launch (start us, length us, event | category | flops | bytes accessed | tf_op | source)
XLA Modules:
  0.0 61.1 jit_solution(12407251343576276040)
XLA Ops:
  0.0 60.3 %shard_map.154 = bf16[256,768]{1,0:T(8,128)(2,1)S(1)} custom-call(bf16[256,768]{1,0:T(8,128)(2,1)} %tok_ref.1, f32[1,3072]{1,0:T(1,128)} %bitcast.8, bf16[384,256]{1,0:T(8,128)(2,1)} %wsi_ref.1, bf16[384,256]{1,0:T(8,128)(2,1)} %wpi_ref.1, f32[64,64]{1,0:T(8,128)} %rr_ref.1, f32[64,64]{1,0:T(8,128)} %ri_ref.1, f32[1,64]{1,0:T(1,128)} %bitcast.11, ...), custom_call_target="tpu_custom_call" | custom-call | tf_op jit(solution)/shard_map/pallas_call | solution.py:1042
  60.3 0.7 %copy.18 = bf16[256,768]{1,0:T(8,128)(2,1)} copy(bf16[256,768]{1,0:T(8,128)(2,1)S(1)} %shard_map.154) | data formatting | bytes 786432

commit v3 on v2

--- a/solution.py
+++ b/solution.py
@@ -458,9 +458,9 @@
     outi_ref, skip_ref, pw_ref, pg_ref, wso_ref, wpo_ref,
     out_ref,
     tok, scaled, squares, w_in, w_out, dmat, rmat, pmat, push, order, halo, halo_out, ends, act,
-    made, rates, matrices, pool_own, dec_ref,
+    guest, partial, sums, made, rates, matrices, pool_own, dec_ref,
     own_sem, xw_send, xw_recv, z_send, z_recv, tok_send, tok_recv, act_send, act_recv, halo_sem, end_send, end_recv,
-    out_send, out_recv,
+    out_send, out_recv, guest_send, guest_recv, guest_z_send, guest_z_recv, part_send, part_recv,
 ):
     me, tp = lax.axis_index("sp"), lax.axis_index("tp")
     n_z = n_sp // n_x
@@ -491,6 +491,12 @@
     def inside(at):
         return jnp.logical_and(at >= 0, at < n_z)
 
+    def inner(at):
+        return jnp.logical_and(at > 0, at < n_z - 1)
+
+    middle, rim = inner(z), jnp.logical_not(inner(z))
+    inward, outward = jnp.where(z == 0, 1, -1), jnp.where(z == 1, -1, 1)
+
     def aligned(index, size):
         return pl.ds(pl.multiple_of(index * size, size), size)
 
@@ -513,27 +519,33 @@
     def out_part(ref, half, j):
         return ref.at[:, pl.ds(pl.multiple_of(half * out_width + j * LANES, LANES), LANES)]
 
-    own_in, own_out = (wsi_ref, wpi_ref), (wso_ref, wpo_ref)
+    own_in, own_out = (wpi_ref, wsi_ref), (wso_ref, wpo_ref)
 
     def in_at(m, sp):
         return w_in.at[m, aligned(sp, in_rows)]
 
-    def out_at(j, m, sp):
-        return w_out.at[j, m, aligned(sp, out_rows)]
+    def out_at(m, sp):
+        return w_out.at[m, :, aligned(sp, out_rows)]
+
+    def weight_at(k, sp):
+        return in_at(k, sp) if k < 2 else out_at(k - 2, sp)
+
+    def parts(k, half, sp):
+        if k < 2:
+            return [(in_part(own_in[k], half), in_at(k, sp))]
+        return [
+            (out_part(own_out[k - 2], half, j), w_out.at[k - 2, j, aligned(sp, out_rows)])
+            for j in range(chunk_count)
+        ]
 
     def own_copy(k):
-        if k < 2:
-            return [pltpu.make_async_copy(in_part(own_in[k], x), in_at(k, me), own_sem.at[k])]
-        return [
-            pltpu.make_async_copy(out_part(own_out[m], x, k - 2), out_at(k - 2, m, me), own_sem.at[k])
-            for m in range(2)
-        ]
+        return [pltpu.make_async_copy(source, there, own_sem.at[k]) for source, there in parts(k, x, me)]
 
     def own_wait(k):
-        here = in_at(k, me) if k < 2 else w_out.at[k - 2, :, aligned(me, out_rows)]
+        here = weight_at(k, me)
         pltpu.make_async_copy(here, here, own_sem.at[k]).wait()
 
-    base = 2 + chunk_count
+    base = 4
     tok_copy = pltpu.make_async_copy(tok_ref, tok.at[tp, aligned(x, rows)], own_sem.at[base])
 
     def heads(ref, count):
@@ -551,93 +563,83 @@
     for c in own_copy(0) + [tok_copy] + loads + [c for k in range(1, base) for c in own_copy(k)]:
         c.start()
 
-    def x_weights(k, sp):
-        if k < 2:
-            return in_part(own_in[k], 1 - x), in_at(k, sp)
-        j, m = (k - 2) // 2, k % 2
-        return out_part(own_out[m], 1 - x, j), out_at(j, m, sp)
-
-    x_kinds = 2 + 2 * chunk_count
-
-    def x_slot(k):
-        return xw_recv.at[k if k < 2 else 2 + (k - 2) // 2]
-
     def x_send(k):
-        return remote(*x_weights(k, me), xw_send.at[0], x_slot(k), to_x)
+        for source, there in parts(k, 1 - x, me):
+            remote(source, there, xw_send.at[0], xw_recv.at[k], to_x).start()
 
     @jax.named_scope("across_wait")
     def x_wait(k):
-        here = in_at(k, beside) if k < 2 else w_out.at[k - 2, :, aligned(beside, out_rows)]
+        here = weight_at(k, beside)
         remote(here, here, xw_send.at[0], xw_recv.at[k], to_x).wait_recv()
 
-    stage_count = 2 + chunk_count
-
     def z_part(stage, h, at):
-        if stage < 2:
-            return in_at(stage, at * n_x + (x if h == 0 else 1 - x))
-        return w_out.at[stage - 2, h, aligned(at, out_rows * n_x)]
+        return weight_at(stage, at * n_x + (x if h == 0 else 1 - x))
+
+    def reach(way, stage):
+        return inside(z + way) if stage < 3 else inner(z + way)
 
     def z_copy(d, stage, s, h):
         at = z - ways[d] * s
         there = z_part(stage, h, at)
         return remote(there, there, z_send.at[d, s], z_recv.at[stage, at, h], to_z(ways[d]))
 
-    def z_own(stage, h):
-        for d in range(2):
-            @pl.when(inside(z + ways[d]))
-            def _():
-                z_copy(d, stage, 0, h).start()
+    def toward(way, stage, inner_side):
+        there = z + way
+        if inner_side:
+            return inner(there)
+        return jnp.logical_and(reach(way, stage), jnp.logical_not(inner(there)))
+
+    def z_own(stage, h, *sides):
+        for inner_side in sides:
+            for d in range(2):
+                @pl.when(toward(ways[d], stage, inner_side))
+                def _():
+                    z_copy(d, stage, 0, h).start()
 
     def z_arrive(d, stage, s, h):
         at = z - ways[d] * (s + 1)
         here = z_part(stage, h, at)
         remote(here, here, z_send.at[d, s], z_recv.at[stage, at, h], to_z(ways[d])).wait_recv()
 
-    @jax.named_scope("relay_wait")
-    def z_relay(stage, s, h):
-        for d in range(2):
-            @pl.when(jnp.logical_and(inside(z - ways[d] * (s + 1)), inside(z + ways[d])))
+    def z_relay(stage, s, h, inner_side, flows):
+        for d in flows:
+            @pl.when(jnp.logical_and(inside(z - ways[d] * (s + 1)), toward(ways[d], stage, inner_side)))
             def _():
                 z_arrive(d, stage, s, h)
                 z_copy(d, stage, s + 1, h).start()
 
+    @jax.named_scope("relay_in")
+    def relay_in(stage, h):
+        z_relay(stage, 0, h, True, range(2))
+
+    @jax.named_scope("relay_out")
+    def relay_out(stage, s, h, flows=(0, 1)):
+        z_relay(stage, s, h, False, flows)
+
     @jax.named_scope("final_wait")
-    def z_final(stage, distances=range(n_z - 1)):
+    def z_final(stage):
+        here = rim if stage < 3 else middle
         for d in range(2):
-            for s in distances:
-                @pl.when(jnp.logical_and(inside(z - ways[d] * (s + 1)), jnp.logical_not(inside(z + ways[d]))))
+            for s in range(n_z - 1):
+                stays = jnp.logical_and(here, jnp.logical_not(reach(ways[d], stage)))
+                @pl.when(jnp.logical_and(inside(z - ways[d] * (s + 1)), stays))
                 def _():
                     for h in range(2):
                         z_arrive(d, stage, s, h)
 
-    def out_own(j):
-        x_wait(2 + j)
-        own_wait(2 + j)
-        for m in range(2):
-            z_own(2 + j, m)
-
-    relays = [(m, 0, h) for h in range(2) for m in range(2)]
-    relays += [(m, s, h) for m in range(2) for s in range(1, n_z - 2) for h in range(2)]
-    in_relays = len(relays)
-    later = [(2 + j, s, m) for j in range(chunk_count) for s in range(n_z - 2) for m in range(2)]
-    relays += sorted(later, key=lambda r: (r[0] > 2, r[1], r[0], r[2]))
-    turn = [0]
-
-    def progress(count=1, stop=None):
-        while count and turn[0] < (len(relays) if stop is None else stop):
-            z_relay(*relays[turn[0]])
-            turn[0] += 1
-            count -= 1
-
     class Gather:
-        def __init__(self, region, pair_region, send, recv):
+        def __init__(self, region, pair_region, send, recv, turned):
             self.region, self.pair_region, self.send, self.recv = region, pair_region, send, recv
+            self.turned = turned
 
         def copy(self, slot, p):
-            at_tp, at_x = ((tp, x), (tp, x), (tp, 1 - x), (tp, x), (tp, 1 - x), (across, x), (across, 1 - x))[slot]
+            at_tp, at_x = (
+                (tp, x), (tp, x), (across, x) if p == self.turned else (tp, 1 - x), (tp, x), (tp, 1 - x), (across, x), (across, 1 - x)
+            )[slot]
             here = self.region(at_tp, at_x, p)
             recv = self.recv.at[2 * slot + p if slot < 3 else 6 if slot < 5 else 7]
-            return remote(here, here, self.send, recv, (to_x, to_y, to_y, to_pair, to_pair, to_pair, to_pair)[slot])
+            target = (to_x, to_y, to_x if p == self.turned else to_y, to_pair, to_pair, to_pair, to_pair)[slot]
+            return remote(here, here, self.send, recv, target)
 
         def start(self, *slots, p):
             for slot in slots:
@@ -655,11 +657,11 @@
 
         def relay_x(self, p):
             self.wait(0, p)
-            self.start(2, 4, p=p)
+            self.start(*((4,) if p == self.turned else (2, 4)), p=p)
 
         def relay_y(self, p):
             self.wait(1, p)
-            self.start(5, p=p)
+            self.start(*((2, 5) if p == self.turned else (5,)), p=p)
 
         def relay_both(self, p):
             self.wait(2, p)
@@ -673,34 +675,44 @@
     def tok_region(at_tp, at_x, p):
         return tok.at[at_tp, pl.ds(pl.multiple_of(at_x * rows + p * piece, piece), piece)]
 
-    tokens = Gather(tok_region, lambda at_tp: tok.at[at_tp], tok_send.at[0], tok_recv)
-
-    def act_gather(which):
-        size = slab // HALVES
-
+    tokens = Gather(tok_region, lambda at_tp: tok.at[at_tp], tok_send.at[0], tok_recv, None)
+
+    half_slab = slab // HALVES
+
+    def act_gather(buffer, send, recv):
         def region(at_tp, at_x, p):
-            return act.at[which, pl.ds(p * size, size), aligned(at_tp * n_x + at_x, width)]
-
-        def pair_region(at_tp):
-            return act.at[which, :, aligned(at_tp, n_x * width)]
-
-        return Gather(region, pair_region, act_send.at[which], act_recv.at[which])
-
-    acts = (act_gather(0), act_gather(1))
+            return buffer.at[pl.ds(p * half_slab, half_slab), aligned(at_tp * n_x + at_x, width)]
+
+        return Gather(region, lambda at_tp: buffer.at[:, aligned(at_tp, n_x * width)], send, recv, 1)
+
+    acts = [act_gather(act.at[k], act_send.at[k], act_recv.at[k]) for k in range(2)]
+    guests = act_gather(guest, guest_send.at[0], guest_recv)
+
+    def guest_copy(p):
+        cut = (pl.ds(p * half_slab, half_slab), aligned(q, width))
+        return remote(
+            act.at[(1, *cut)], guest.at[cut], guest_z_send.at[0], guest_z_recv.at[p], to_z(inward)
+        )
+
+    def part_rows(j, first):
+        return partial.at[j, aligned(1 - x if first else x, rows)]
+
+    def part_copy(j, first):
+        here = part_rows(j, first)
+        return remote(here, here, part_send.at[0], part_recv.at[j, 0 if first else 1], to_z(outward))
 
     pl.semaphore_wait(barrier, 3 + inside(z + 1).astype(jnp.int32) + inside(z - 1).astype(jnp.int32))
 
-    x_send(0).start()
+    both_sides = (True, False)
+    x_send(0)
     own_wait(0)
-    z_own(0, 0)
+    z_own(0, 0, *both_sides)
     own_wait(1)
-    z_own(1, 0)
-    x_send(1).start()
+    z_own(1, 0, *both_sides)
     tok_copy.wait()
     for p in range(HALVES):
         tokens.start(0, 1, 3, p=p)
-    for k in range(2, x_kinds):
-        x_send(k).start()
+    x_send(1)
 
     tile = iota((states, columns), 0) == iota((states, columns), 1) % states
     tile_exact, tile_half = tile.astype(f32), tile.astype(bf16)
@@ -791,42 +803,110 @@
 
     build_decay()
     build_drive(0)
-    progress()
+    relay_in(0, 0)
+    relay_out(0, 0, 0)
     x_wait(0)
-    z_own(0, 1)
-    progress()
+    z_own(0, 1, *both_sides)
+    relay_in(1, 0)
+    tokens.relay_y(0)
+    build_drive(1)
+    relay_out(0, 1, 0)
+    build_read(0)
+    relay_in(0, 1)
+    relay_out(0, 0, 1)
+    tokens.relay_x(0)
+    tokens.relay_y(1)
+    own_wait(2)
+    own_wait(3)
+    z_own(2, 0, True)
+    build_read(1)
+    relay_out(1, 0, 0)
+    build_order(0)
+    build_order(1)
+    build_pool()
+    relay_out(0, 1, 1)
+    tokens.relay_x(1)
     x_wait(1)
-    z_own(1, 1)
-    build_drive(1)
-    build_read(0)
-    progress()
-    build_read(1)
-    progress()
-    tokens.relay_x(0)
-    build_order(0)
-    progress()
-    build_pool()
-    tokens.relay_y(0)
-    tokens.relay_x(1)
-    progress()
-    build_order(1)
-    progress(stop=in_relays)
-    tokens.relay_y(1)
+    z_own(1, 1, *both_sides)
+    x_send(2)
+    x_send(3)
+    z_own(3, 0, True)
+    relay_out(1, 1, 0)
+    take(tp, True)
+    tokens.relay_both(0)
     tokens.wait_pair(pair, 0)
-    take(tp, True)
-    progress(stop=in_relays)
     take(pair, False)
-    progress(stop=in_relays)
-    tokens.relay_both(0)
-    out_own(0)
+    relay_in(1, 1)
     tokens.relay_both(1)
+    relay_in(2, 0)
     take(across, False)
+    relay_out(1, 0, 1)
     tokens.wait_pair(both, 1)
     take(both, False)
-    progress(2)
+    relay_out(1, 1, 1, (1,))
     inverse = lax.rsqrt(squares[...] / (features * n_tp) + epsilon)
     z_final(0)
-    state_in = (dot(scaled[...], w_in[0]) * inverse).astype(bf16)
+    pool_in = (dot(scaled[...], w_in[0]) * inverse).astype(bf16)
+    halo_out[...] = pool_in[slab - window_reach :]
+    halo_copy = remote(halo_out, halo, halo_sem.at[0], halo_sem.at[1], to_z(1))
+
+    @pl.when(inside(z + 1))
+    def _():
+        halo_copy.start()
+
+    relay_out(1, 1, 1, (0,))
+    relay_in(3, 0)
+
+    @pl.when(rim)
+    def _():
+        x_wait(2)
+        z_own(2, 1, True)
+
+
+    @pl.when(z > 0)
+    @jax.named_scope("halo_wait")
+    def _():
+        halo_copy.wait_recv()
+
+    before = jnp.where(z == 0, jnp.zeros_like(halo), halo[...])
+    whole = jnp.concatenate([before, pool_in], axis=0).astype(f32)
+    window = jnp.left_shift(2, (q * pool_groups + iota((slab, width), 1) // POOL_GROUP) % 4)
+    window_sums = jnp.zeros((slab, width), f32)
+    running = whole
+    for level in range(4):
+        running = running + pltpu.roll(running, 2**level, 0)
+        window_sums = jnp.where(window == 2 ** (level + 1), running[window_reach:], window_sums)
+    position = z * slab + iota((slab, width), 0)
+    divisor = jnp.minimum(position + 1, window).astype(f32)
+    pooled = window_sums / divisor - whole[window_reach:]
+    pooled_high, pooled_low = split(pooled)
+    pool_gain = pg_ref[:, aligned(q, width)]
+    projected = dot(pooled_high, pmat[...]) + dot(pooled_low, pmat[...])
+    act[1, :, aligned(q, width)] = (projected * pool_gain).astype(bf16)
+
+    @pl.when(rim)
+    def _():
+        for p in range(HALVES):
+            guest_copy(p).start()
+
+    @pl.when(middle)
+    def _():
+        for p in range(HALVES):
+            acts[1].start(0, 1, 3, p=p)
+
+    z_own(2, 0, False)
+
+    @pl.when(middle)
+    def _():
+        x_wait(2)
+        z_own(2, 1, *both_sides)
+
+    x_wait(3)
+    z_own(3, 1, True)
+    relay_out(2, 0, 0)
+    z_final(1)
+    state_in = (dot(scaled[...], w_in[1]) * inverse).astype(bf16)
+    relay_in(2, 1)
     signal = dot(order[0], state_in).astype(bf16)
     for i in range(2):
         push[i] = dot(signal, dmat[i, 0]) + dot(signal, dmat[i, 1])
@@ -871,20 +951,38 @@
         def _():
             end_copy(k).start()
 
-    if chunk_count > 1:
-        out_own(1)
-    z_final(1)
-    pool_in = (dot(scaled[...], w_in[1]) * inverse).astype(bf16)
-    halo_out[...] = pool_in[slab - window_reach :]
-    halo_copy = remote(halo_out, halo, halo_sem.at[0], halo_sem.at[1], to_z(1))
-
-    @pl.when(inside(z + 1))
-    def _():
-        halo_copy.start()
-
-    progress(2)
-    for j in range(2, chunk_count):
-        out_own(j)
+    @pl.when(middle)
+    def _():
+        for p in range(HALVES):
+            here = guests.region(tp, x, p)
+            with jax.named_scope("guest_wait"):
+                remote(here, here, guest_z_send.at[0], guest_z_recv.at[p], to_pair).wait_recv()
+            guests.start(0, 1, 3, p=p)
+
+    relay_out(2, 1, 0)
+    relay_out(2, 0, 1)
+
+    @pl.when(middle)
+    def _():
+        for p in range(HALVES):
+            acts[1].relay_x(p)
+            acts[1].relay_y(p)
+
+    @pl.when(middle)
+    def _():
+        for p in range(HALVES):
+            acts[1].relay_both(p)
+
+    relay_in(3, 1)
+
+    @pl.when(middle)
+    def _():
+        for p in range(HALVES):
+            guests.relay_x(p)
+            guests.relay_y(p)
+
+    relay_out(2, 1, 1)
+
     for k in range(1, n_z):
         @pl.when(inside(z - k))
         @jax.named_scope("ends_wait")
@@ -915,7 +1013,6 @@
         return real, imag
 
     lax.fori_loop(0, span, add_carry, (begin_real, begin_imag), unroll=4)
-    progress(2)
     real_high, real_low = split(push[0])
     imag_high, imag_low = split(push[1])
     readout = dot(real_high, rmat[0, 0]) + dot(real_high, rmat[0, 1]) + dot(real_low, rmat[0, 0])
@@ -926,44 +1023,38 @@
     act[0, :, aligned(q, width)] = dot(order[1], shuffled).astype(bf16)
     for p in range(HALVES):
         acts[0].start(0, 1, 3, p=p)
-    progress(2)
-
-    @pl.when(z > 0)
-    @jax.named_scope("halo_wait")
-    def _():
-        halo_copy.wait_recv()
-
-    before = jnp.where(z == 0, jnp.zeros_like(halo), halo[...])
-    whole = jnp.concatenate([before, pool_in], axis=0).astype(f32)
-    window = jnp.left_shift(2, (q * pool_groups + iota((slab, width), 1) // POOL_GROUP) % 4)
-    sums = jnp.zeros((slab, width), f32)
-    running = whole
-    for level in range(4):
-        running = running + pltpu.roll(running, 2**level, 0)
-        sums = jnp.where(window == 2 ** (level + 1), running[window_reach:], sums)
-    position = z * slab + iota((slab, width), 0)
-    divisor = jnp.minimum(position + 1, window).astype(f32)
-    pooled = sums / divisor - whole[window_reach:]
-    pooled_high, pooled_low = split(pooled)
-    pool_gain = pg_ref[:, aligned(q, width)]
-    projected = dot(pooled_high, pmat[...]) + dot(pooled_low, pmat[...])
-    act[1, :, aligned(q, width)] = (projected * pool_gain).astype(bf16)
+
+    @pl.when(middle)
+    def _():
+        for p in range(HALVES):
+            guests.relay_both(p)
+        guests.wait_pair(pair, 0)
+        guests.wait_pair(both, 1)
+
+    z_final(3)
+
+    @pl.when(middle)
+    def _():
+        for first in (True, False):
+            cut = aligned(1 - x if first else x, rows)
+            for j in range(chunk_count):
+                partial[j, cut] = dot(guest[cut], w_out[1, j]).astype(bf16)
+                part_copy(j, first).start()
+
     for p in range(HALVES):
-        acts[1].start(0, 1, 3, p=p)
-    progress(2)
-    for k in range(2):
-        for p in range(HALVES):
-            acts[k].relay_x(p)
-            acts[k].relay_y(p)
-            progress()
-    for k in range(2):
-        for p in range(HALVES):
-            acts[k].relay_both(p)
-            progress()
-    progress(len(relays))
-    for k in range(2):
-        acts[k].wait_pair(pair, 0)
-        acts[k].wait_pair(both, 1)
+        acts[0].relay_x(p)
+        acts[0].relay_y(p)
+    for p in range(HALVES):
+        acts[0].relay_both(p)
+
+    @pl.when(middle)
+    def _():
+        acts[1].wait_pair(pair, 0)
+        acts[1].wait_pair(both, 1)
+
+    acts[0].wait_pair(pair, 0)
+    acts[0].wait_pair(both, 1)
+    z_final(2)
 
     def out_columns(half, j):
         return pl.ds(pl.multiple_of(half * out_width + j * LANES, LANES), LANES)
@@ -971,44 +1062,64 @@
     def out_copy(j):
         return remote(made.at[j], out_ref.at[:, out_columns(x, j)], out_send.at[0], out_recv.at[0], to_x)
 
-    def part(j, half, at):
-        cut, depth = aligned(half, rows), aligned(at, n_x * out_rows)
-        return dot(act[0, cut, depth], w_out[j, 0, depth]) + dot(act[1, cut, depth], w_out[j, 1, depth])
-
-    def make(j, half):
-        cut = aligned(half, rows)
-        return dot(act[0, cut], w_out[j, 0]) + dot(act[1, cut], w_out[j, 1])
-
-    for j in range(chunk_count):
-        if j + 1 < chunk_count:
-            z_final(2 + j)
-            made[j] = make(j, 1 - x).astype(bf16)
+    here, there = aligned(x, rows), aligned(1 - x, rows)
+
+    @pl.when(middle)
+    def _():
+        for j in range(chunk_count):
+            made[j] = (dot(act[0, there], w_out[0, j]) + dot(act[1, there], w_out[1, j])).astype(bf16)
             out_copy(j).start()
-            out_ref[:, out_columns(x, j)] = make(j, x).astype(bf16)
-        else:
-            far = n_z - 1 - z
-            z_final(2 + j, range(n_z - 2))
-            sums = [
-                sum(part(j, half, (far + 1 + r) % n_z) for r in range(n_z - 1)) for half in (1 - x, x)
-            ]
-            z_final(2 + j, range(n_z - 2, n_z - 1))
-            made[j] = (sums[0] + part(j, 1 - x, far)).astype(bf16)
+        for j in range(chunk_count):
+            mine = dot(act[0, here], w_out[0, j]) + dot(act[1, here], w_out[1, j])
+            out_ref[:, out_columns(x, j)] = mine.astype(bf16)
+
+    @pl.when(rim)
+    def _():
+        for cut in (there, here):
+            for j in range(chunk_count):
+                sums[j, cut] = dot(act[0, cut], w_out[0, j])
+
+        @jax.named_scope("partial_wait")
+        def part_wait(j, first):
+            part = part_rows(j, first)
+            recv = part_recv.at[j, 0 if first else 1]
+            remote(part, part, part_send.at[0], recv, to_pair).wait_recv()
+
+        for j in range(chunk_count):
+            part_wait(j, True)
+            made[j] = (sums[j, there] + partial[j, there].astype(f32)).astype(bf16)
             out_copy(j).start()
-            out_ref[:, out_columns(x, j)] = (sums[1] + part(j, x, far)).astype(bf16)
+        for j in range(chunk_count):
+            part_wait(j, False)
+            out_ref[:, out_columns(x, j)] = (sums[j, here] + partial[j, here].astype(f32)).astype(bf16)
 
     @jax.named_scope("drain")
     def drain():
         sent = w_in.at[0, pl.ds(0, 2 * in_rows + 2 * chunk_count * out_rows)]
         remote(sent, sent, xw_send.at[0], xw_recv.at[0], to_x).wait_send()
-        sent = w_in.at[0, pl.ds(0, n_x * (2 * in_rows + 2 * chunk_count * out_rows))]
+        few = n_x * (2 * in_rows + chunk_count * out_rows)
+        many = few + n_x * chunk_count * out_rows
         for d in range(2):
             for s in range(n_z - 1):
-                @pl.when(jnp.logical_and(inside(z + ways[d]), inside(z - ways[d] * s)))
-                def _():
-                    remote(sent, sent, z_send.at[d, s], z_recv.at[0, 0, 0], to_z(ways[d])).wait_send()
+                any_sent = jnp.logical_and(inside(z + ways[d]), inside(z - ways[d] * s))
+                for count, case in ((many, inner(z + ways[d])), (few, jnp.logical_not(inner(z + ways[d])))):
+                    @pl.when(jnp.logical_and(any_sent, case))
+                    def _():
+                        sent = w_in.at[0, pl.ds(0, count)]
+                        remote(sent, sent, z_send.at[d, s], z_recv.at[0, 0, 0], to_z(ways[d])).wait_send()
         tokens.drain(scaled.at[pl.ds(0, 7 * rows // n_tp)])
-        for k in range(2):
-            acts[k].drain(act.at[k, :, pl.ds(0, 7 * width)])
+        acts[0].drain(act.at[0, :, pl.ds(0, 7 * width)])
+
+        @pl.when(middle)
+        def _():
+            acts[1].drain(act.at[1, :, pl.ds(0, 7 * width)])
+            guests.drain(guest.at[:, pl.ds(0, 7 * width)])
+            remote(partial, partial, part_send.at[0], part_recv.at[0, 0], to_pair).wait_send()
+
+        @pl.when(rim)
+        def _():
+            sent = act.at[1, :, aligned(q, width)]
+            remote(sent, sent, guest_z_send.at[0], guest_z_recv.at[0], to_pair).wait_send()
 
         @pl.when(inside(z + 1))
         def _():
@@ -1050,7 +1161,7 @@
             pltpu.VMEM((slab, features * n_tp), bf16),
             pltpu.VMEM((slab, LANES), f32),
             pltpu.VMEM((2, n_sp * in_rows, width), bf16),
-            pltpu.VMEM((chunk_count, 2, n_sp * out_rows, LANES), bf16),
+            pltpu.VMEM((2, chunk_count, n_sp * out_rows, LANES), bf16),
             pltpu.VMEM((2, 2, width, columns), bf16),
             pltpu.VMEM((2, 2, columns, width), bf16),
             pltpu.VMEM((width, width), bf16),
@@ -1060,16 +1171,19 @@
             pltpu.VMEM((window_reach, width), bf16),
             pltpu.VMEM((n_z, CHUNKS, columns), f32),
             pltpu.VMEM((2, slab, n_tp * n_x * width), bf16),
+            pltpu.VMEM((slab, n_tp * n_x * width), bf16),
+            pltpu.VMEM((chunk_count, slab, LANES), bf16),
+            pltpu.VMEM((chunk_count, slab, LANES), f32),
             pltpu.VMEM((chunk_count, rows, LANES), bf16),
             pltpu.VMEM((2, groups, states), f32),
             pltpu.VMEM((4, groups, SSM_GROUP, states), f32),
             pltpu.VMEM((pool_groups, POOL_GROUP, POOL_GROUP), bf16),
             pltpu.VMEM((2, columns), f32),
-            dma((6 + chunk_count,)),
+            dma((8,)),
             dma((1,)),
-            dma((2 + chunk_count,)),
+            dma((4,)),
             dma((2, n_z - 1)),
-            dma((2 + chunk_count, n_z, 2)),
+            dma((4, n_z, 2)),
             dma((1,)),
             dma((8,)),
             dma((2,)),
@@ -1079,6 +1193,12 @@
             dma((n_z - 1,)),
             dma((1,)),
             dma((1,)),
+            dma((1,)),
+            dma((8,)),
+            dma((1,)),
+            dma((HALVES,)),
+            dma((1,)),
+            dma((chunk_count, 2)),
         ],
         compiler_params=pltpu.CompilerParams(
             collective_id=0, has_side_effects=True, vmem_limit_bytes=60 * 2**20
@@ -1088,7 +1208,7 @@
 
 def slab_fits(n_sp, n_tp, n_x, in_rows, width, pool_width, out_rows, out_columns):
     return (
-        n_x == 2 and n_tp == 4 and n_sp // n_x >= 3 and width == n_x * LANES
+        n_x == 2 and n_tp == 4 and n_sp // n_x == 4 and width == n_x * LANES
         and pool_width == width and out_columns % (n_x * LANES) == 0
         and n_x * (2 * in_rows + out_columns // (n_x * LANES) * 2 * out_rows) <= n_sp * in_rows
     )

time: 62.1 us -> 59.8 us (0.963)
  Pallas kernels: 60.3 us -> 58.2 us
    pallas_call x1, Pallas kernels: 60.3 us -> 58.2 us  [slab_call(): pl.pallas_call(functools.partial(slab_kernel, n_sp, n_tp, n_x, states), o...]
where the time goes in v3:
time: 59.8 us; the launch traced here: 59 us
  Pallas kernels  58.2 us (97%)
  local copies, waits for them, and re-layouts  0.75 us (1%)
    pallas_call x1, Pallas kernels, slab_call(): pl.pallas_call(functools.partial(slab_kernel, n_sp, n_tp, n_x, states), o...  58.2 us

profile of v3, /device:TPU:17, one launch (start us, length us, event | category | flops | bytes accessed | tf_op | source)
XLA Modules:
  0.0 59.0 jit_solution(6341898504379365894)
XLA Ops:
  0.0 58.2 %shard_map.154 = bf16[256,768]{1,0:T(8,128)(2,1)S(1)} custom-call(bf16[256,768]{1,0:T(8,128)(2,1)} %tok_ref.1, f32[1,3072]{1,0:T(1,128)} %bitcast.8, bf16[384,256]{1,0:T(8,128)(2,1)} %wsi_ref.1, bf16[384,256]{1,0:T(8,128)(2,1)} %wpi_ref.1, f32[64,64]{1,0:T(8,128)} %rr_ref.1, f32[64,64]{1,0:T(8,128)} %ri_ref.1, f32[1,64]{1,0:T(1,128)} %bitcast.11, ...), custom_call_target="tpu_custom_call" | custom-call | tf_op jit(solution)/shard_map/pallas_call | solution.py:1153
  58.2 0.7 %copy.18 = bf16[256,768]{1,0:T(8,128)(2,1)} copy(bf16[256,768]{1,0:T(8,128)(2,1)S(1)} %shard_map.154) | data formatting | bytes 786432

commit v4 on v3

--- a/solution.py
+++ b/solution.py
@@ -589,9 +589,9 @@
             return inner(there)
         return jnp.logical_and(reach(way, stage), jnp.logical_not(inner(there)))
 
-    def z_own(stage, h, *sides):
+    def z_own(stage, h, *sides, flows=(0, 1)):
         for inner_side in sides:
-            for d in range(2):
+            for d in flows:
                 @pl.when(toward(ways[d], stage, inner_side))
                 def _():
                     z_copy(d, stage, 0, h).start()
@@ -609,8 +609,8 @@
                 z_copy(d, stage, s + 1, h).start()
 
     @jax.named_scope("relay_in")
-    def relay_in(stage, h):
-        z_relay(stage, 0, h, True, range(2))
+    def relay_in(stage, h, flows=(0, 1)):
+        z_relay(stage, 0, h, True, flows)
 
     @jax.named_scope("relay_out")
     def relay_out(stage, s, h, flows=(0, 1)):
@@ -794,7 +794,8 @@
         def step(i, _):
             here = pl.ds(pl.multiple_of(i * size, size), size)
             block = tok[at_tp, here].astype(f32)
-            total = jnp.broadcast_to(jnp.sum(block * block, axis=1, keepdims=True), (size, LANES))
+            square = block * block
+            total = sum(square[:, k : k + LANES] for k in range(0, features, LANES))
             squares[here] = total if first else squares[here] + total
             scaled[here, cut] = (block * gain).astype(bf16)
             return 0
@@ -828,8 +829,8 @@
     tokens.relay_x(1)
     x_wait(1)
     z_own(1, 1, *both_sides)
+    x_send(3)
     x_send(2)
-    x_send(3)
     z_own(3, 0, True)
     relay_out(1, 1, 0)
     take(tp, True)
@@ -843,8 +844,7 @@
     relay_out(1, 0, 1)
     tokens.wait_pair(both, 1)
     take(both, False)
-    relay_out(1, 1, 1, (1,))
-    inverse = lax.rsqrt(squares[...] / (features * n_tp) + epsilon)
+    inverse = lax.rsqrt(jnp.sum(squares[...], axis=1, keepdims=True) / (features * n_tp) + epsilon)
     z_final(0)
     pool_in = (dot(scaled[...], w_in[0]) * inverse).astype(bf16)
     halo_out[...] = pool_in[slab - window_reach :]
@@ -854,13 +854,13 @@
     def _():
         halo_copy.start()
 
-    relay_out(1, 1, 1, (0,))
+    relay_out(1, 1, 1)
     relay_in(3, 0)
 
     @pl.when(rim)
     def _():
-        x_wait(2)
-        z_own(2, 1, True)
+        x_wait(3)
+        z_own(3, 1, True)
 
 
     @pl.when(z > 0)
@@ -896,17 +896,22 @@
 
     z_own(2, 0, False)
 
+    x_wait(2)
+
+    @pl.when(rim)
+    def _():
+        z_own(2, 1, True)
+
     @pl.when(middle)
     def _():
-        x_wait(2)
-        z_own(2, 1, *both_sides)
-
-    x_wait(3)
-    z_own(3, 1, True)
-    relay_out(2, 0, 0)
+        x_wait(3)
+        z_own(2, 1, True, False, flows=(1,))
+        z_own(3, 1, True, flows=(1,))
+
+    relay_out(2, 0, 0, (1,))
     z_final(1)
     state_in = (dot(scaled[...], w_in[1]) * inverse).astype(bf16)
-    relay_in(2, 1)
+    relay_in(3, 1, (1,))
     signal = dot(order[0], state_in).astype(bf16)
     for i in range(2):
         push[i] = dot(signal, dmat[i, 0]) + dot(signal, dmat[i, 1])
@@ -959,8 +964,14 @@
                 remote(here, here, guest_z_send.at[0], guest_z_recv.at[p], to_pair).wait_recv()
             guests.start(0, 1, 3, p=p)
 
+    @pl.when(middle)
+    def _():
+        z_own(2, 1, True, False, flows=(0,))
+        z_own(3, 1, True, flows=(0,))
+
+    relay_in(3, 1, (0,))
+    relay_out(2, 0, 0, (0,))
     relay_out(2, 1, 0)
-    relay_out(2, 0, 1)
 
     @pl.when(middle)
     def _():
@@ -968,20 +979,20 @@
             acts[1].relay_x(p)
             acts[1].relay_y(p)
 
+    relay_in(2, 1)
+    relay_out(2, 0, 1, (1,))
+
     @pl.when(middle)
     def _():
         for p in range(HALVES):
             acts[1].relay_both(p)
 
-    relay_in(3, 1)
 
     @pl.when(middle)
     def _():
         for p in range(HALVES):
             guests.relay_x(p)
             guests.relay_y(p)
-
-    relay_out(2, 1, 1)
 
     for k in range(1, n_z):
         @pl.when(inside(z - k))
@@ -1023,6 +1034,9 @@
     act[0, :, aligned(q, width)] = dot(order[1], shuffled).astype(bf16)
     for p in range(HALVES):
         acts[0].start(0, 1, 3, p=p)
+
+    relay_out(2, 0, 1, (0,))
+    relay_out(2, 1, 1)
 
     @pl.when(middle)
     def _():
@@ -1206,9 +1220,9 @@
     )(*arrays)
 
 
-def slab_fits(n_sp, n_tp, n_x, in_rows, width, pool_width, out_rows, out_columns):
+def slab_fits(n_sp, n_tp, n_x, features, in_rows, width, pool_width, out_rows, out_columns):
     return (
-        n_x == 2 and n_tp == 4 and n_sp // n_x == 4 and width == n_x * LANES
+        n_x == 2 and n_tp == 4 and n_sp // n_x == 4 and features % LANES == 0 and width == n_x * LANES
         and pool_width == width and out_columns % (n_x * LANES) == 0
         and n_x * (2 * in_rows + out_columns // (n_x * LANES) * 2 * out_rows) <= n_sp * in_rows
     )
@@ -1228,7 +1242,7 @@
     states = rate_real.shape[1]
     columns = groups * states
     pool_groups = pool_width // POOL_GROUP
-    if slab_fits(n_sp, n_tp, n_x, in_rows, width, pool_width, out_rows, out_columns):
+    if slab_fits(n_sp, n_tp, n_x, features, in_rows, width, pool_width, out_rows, out_columns):
         return slab_call(n_sp, n_tp, n_x, (
             tokens, norm_gain[None], state_in_weight, pool_in_weight, rate_real, rate_imag, log_step[None],
             jnp.swapaxes(input_real, 1, 2), jnp.swapaxes(input_imag, 1, 2), output_real, output_imag,

time: 59.8 us -> 58.6 us (0.980); the launches traced: 59 us -> 58.4 us
  no operation moved by 1% of the time
where the time goes in v4:
time: 58.6 us; the launch traced here: 58.4 us
  Pallas kernels  57.7 us (98%)
  local copies, waits for them, and re-layouts  0.75 us (1%)
    pallas_call x1, Pallas kernels, slab_call(): pl.pallas_call(functools.partial(slab_kernel, n_sp, n_tp, n_x, states), o...  57.7 us

profile of v4, /device:TPU:17, one launch (start us, length us, event | category | flops | bytes accessed | tf_op | source)
XLA Modules:
  0.0 58.4 jit_solution(16660039047984994229)
XLA Ops:
  0.0 57.7 %shard_map.154 = bf16[256,768]{1,0:T(8,128)(2,1)S(1)} custom-call(bf16[256,768]{1,0:T(8,128)(2,1)} %tok_ref.1, f32[1,3072]{1,0:T(1,128)} %bitcast.8, bf16[384,256]{1,0:T(8,128)(2,1)} %wsi_ref.1, bf16[384,256]{1,0:T(8,128)(2,1)} %wpi_ref.1, f32[64,64]{1,0:T(8,128)} %rr_ref.1, f32[64,64]{1,0:T(8,128)} %ri_ref.1, f32[1,64]{1,0:T(1,128)} %bitcast.11, ...), custom_call_target="tpu_custom_call" | custom-call | tf_op jit(solution)/shard_map/pallas_call | solution.py:1167
  57.7 0.7 %copy.18 = bf16[256,768]{1,0:T(8,128)(2,1)} copy(bf16[256,768]{1,0:T(8,128)(2,1)S(1)} %shard_map.154) | data formatting | bytes 786432

commit v5 on v4

--- a/solution.py
+++ b/solution.py
@@ -863,6 +863,13 @@
         z_own(3, 1, True)
 
 
+    def project_state():
+        sums[0] = (dot(scaled[...], w_in[1]) * inverse).astype(bf16).astype(f32)
+
+    @pl.when(middle)
+    def _():
+        project_state()
+
     @pl.when(z > 0)
     @jax.named_scope("halo_wait")
     def _():
@@ -910,7 +917,12 @@
 
     relay_out(2, 0, 0, (1,))
     z_final(1)
-    state_in = (dot(scaled[...], w_in[1]) * inverse).astype(bf16)
+
+    @pl.when(rim)
+    def _():
+        project_state()
+
+    state_in = sums[0].astype(bf16)
     relay_in(3, 1, (1,))
     signal = dot(order[0], state_in).astype(bf16)
     for i in range(2):
@@ -1058,13 +1070,15 @@
     for p in range(HALVES):
         acts[0].relay_x(p)
         acts[0].relay_y(p)
+        if p == 0:
+            @pl.when(middle)
+            def _():
+                acts[1].wait_pair(pair, 0)
+                acts[1].wait_pair(both, 1)
+                for j in range(chunk_count):
+                    sums[j] = dot(act[1], w_out[1, j])
     for p in range(HALVES):
         acts[0].relay_both(p)
-
-    @pl.when(middle)
-    def _():
-        acts[1].wait_pair(pair, 0)
-        acts[1].wait_pair(both, 1)
 
     acts[0].wait_pair(pair, 0)
     acts[0].wait_pair(both, 1)
@@ -1081,10 +1095,10 @@
     @pl.when(middle)
     def _():
         for j in range(chunk_count):
-            made[j] = (dot(act[0, there], w_out[0, j]) + dot(act[1, there], w_out[1, j])).astype(bf16)
+            made[j] = (dot(act[0, there], w_out[0, j]) + sums[j, there]).astype(bf16)
             out_copy(j).start()
         for j in range(chunk_count):
-            mine = dot(act[0, here], w_out[0, j]) + dot(act[1, here], w_out[1, j])
+            mine = dot(act[0, here], w_out[0, j]) + sums[j, here]
             out_ref[:, out_columns(x, j)] = mine.astype(bf16)
 
     @pl.when(rim)

time: 58.6 us -> 57.5 us (0.981)
  Pallas kernels: 57.7 us -> 56.2 us
    pallas_call x1, Pallas kernels: 57.7 us -> 56.2 us  [slab_call(): pl.pallas_call(functools.partial(slab_kernel, n_sp, n_tp, n_x, states), o...]
where the time goes in v5:
time: 57.5 us; the launch traced here: 56.9 us
  Pallas kernels  56.2 us (98%)
  local copies, waits for them, and re-layouts  0.75 us (1%)
    pallas_call x1, Pallas kernels, slab_call(): pl.pallas_call(functools.partial(slab_kernel, n_sp, n_tp, n_x, states), o...  56.2 us

profile of v5, /device:TPU:17, one launch (start us, length us, event | category | flops | bytes accessed | tf_op | source)
XLA Modules:
  0.0 56.9 jit_solution(17337012056748074928)
XLA Ops:
  0.0 56.2 %shard_map.154 = bf16[256,768]{1,0:T(8,128)(2,1)S(1)} custom-call(bf16[256,768]{1,0:T(8,128)(2,1)} %tok_ref.1, f32[1,3072]{1,0:T(1,128)} %bitcast.8, bf16[384,256]{1,0:T(8,128)(2,1)} %wsi_ref.1, bf16[384,256]{1,0:T(8,128)(2,1)} %wpi_ref.1, f32[64,64]{1,0:T(8,128)} %rr_ref.1, f32[64,64]{1,0:T(8,128)} %ri_ref.1, f32[1,64]{1,0:T(1,128)} %bitcast.11, ...), custom_call_target="tpu_custom_call" | custom-call | tf_op jit(solution)/shard_map/pallas_call | solution.py:1181
  56.2 0.7 %copy.18 = bf16[256,768]{1,0:T(8,128)(2,1)} copy(bf16[256,768]{1,0:T(8,128)(2,1)S(1)} %shard_map.154) | data formatting | bytes 786432

commit v6 on v5

--- a/solution.py
+++ b/solution.py
@@ -811,6 +811,7 @@
     relay_in(1, 0)
     tokens.relay_y(0)
     build_drive(1)
+    relay_out(1, 0, 0)
     relay_out(0, 1, 0)
     build_read(0)
     relay_in(0, 1)
@@ -821,7 +822,6 @@
     own_wait(3)
     z_own(2, 0, True)
     build_read(1)
-    relay_out(1, 0, 0)
     build_order(0)
     build_order(1)
     build_pool()

time: 57.5 us -> 57.5 us (level)
  no operation moved by 1% of the time
where the time goes in v6:
time: 57.5 us; the launch traced here: 56.9 us
  Pallas kernels  56.2 us (98%)
  local copies, waits for them, and re-layouts  0.75 us (1%)
    pallas_call x1, Pallas kernels, slab_call(): pl.pallas_call(functools.partial(slab_kernel, n_sp, n_tp, n_x, states), o...  56.2 us

profile of v6, /device:TPU:17, one launch (start us, length us, event | category | flops | bytes accessed | tf_op | source)
XLA Modules:
  0.0 56.9 jit_solution(907835269758587233)
XLA Ops:
  0.0 56.2 %shard_map.154 = bf16[256,768]{1,0:T(8,128)(2,1)S(1)} custom-call(bf16[256,768]{1,0:T(8,128)(2,1)} %tok_ref.1, f32[1,3072]{1,0:T(1,128)} %bitcast.8, bf16[384,256]{1,0:T(8,128)(2,1)} %wsi_ref.1, bf16[384,256]{1,0:T(8,128)(2,1)} %wpi_ref.1, f32[64,64]{1,0:T(8,128)} %rr_ref.1, f32[64,64]{1,0:T(8,128)} %ri_ref.1, f32[1,64]{1,0:T(1,128)} %bitcast.11, ...), custom_call_target="tpu_custom_call" | custom-call | tf_op jit(solution)/shard_map/pallas_call | solution.py:1181
  56.2 0.7 %copy.18 = bf16[256,768]{1,0:T(8,128)(2,1)} copy(bf16[256,768]{1,0:T(8,128)(2,1)S(1)} %shard_map.154) | data formatting | bytes 786432
